TPU v7x, 128 devices: a whole 4x4x4 slice. The times are simulated.
128 devices in a mesh: pp: 4 (over x), fs: 4 (over y), tp: 8 (over z, core).
Axes of the slice: x: 4, y: 4, z: 4, core: 2. Of those that a mesh axis runs over, the one named last changes fastest.
Arguments:
- micro_in: bfloat16 [2, 96, 1024], P(None, 'pp', ('tp', 'fs')), may hold values from -6 to 6
- norm_gain: float32 [4, 1024], P('pp'), may hold values from 0.5 to 1.5
- proj_gate: bfloat16 [4, 1024, 8, 4, 64], P('pp', None, 'tp', 'fs'), may hold values from -0.1875 to 0.1875
- proj_value: bfloat16 [4, 1024, 8, 4, 64], P('pp', None, 'tp', 'fs'), may hold values from -0.1875 to 0.1875
- proj_write: bfloat16 [4, 1024, 8, 128], P('pp', None, 'tp'), may hold values from -0.1875 to 0.1875
- proj_read: bfloat16 [4, 1024, 8, 128], P('pp', None, 'tp'), may hold values from -0.1875 to 0.1875
- proj_step: bfloat16 [4, 1024, 2, 8, 4], P('pp', None, None, 'tp', 'fs'), may hold values from -0.1875 to 0.1875
- step_bias: float32 [4, 2, 8, 4], P('pp', None, 'tp', 'fs'), may hold values from -4.6 to -2.3
- decay_log: float32 [4, 2, 8, 4], P('pp', None, 'tp', 'fs'), may hold values from 0 to 2.77
- skip_gain: float32 [4, 8, 4], P('pp', 'tp', 'fs'), may hold values from 0.5 to 1.5
- conv_value: float32 [4, 5, 8, 4, 64], P('pp', None, 'tp', 'fs'), may hold values from -2.5 to 2.5
- conv_write: float32 [4, 5, 8, 128], P('pp', None, 'tp'), may hold values from -2.5 to 2.5
- conv_read: float32 [4, 5, 8, 128], P('pp', None, 'tp'), may hold values from -2.5 to 2.5
- proj_out: bfloat16 [4, 8, 4, 64, 1024], P('pp', 'tp', 'fs'), may hold values from -0.125 to 0.125
Outputs:
- mixed_out: bfloat16 [2, 96, 1024], P(None, 'pp', ('tp', 'fs'))
All inputs are finite; a program needn't handle non-finite values.
Results may differ from a plain program's by a relative error of at most 0.025.
Values may be sent and summed in bfloat16 or wider, within the bound.
No kernel may reach another device: no remote copies, remote signals or barrier semaphores. Data moves between devices by JAX's collectives and lax.ppermute only.
A program may use at most 64 MiB of HBM per device.

v0:
```python
import jax
import jax.numpy as jnp
from jax import lax
from jax.experimental import pallas as pl
from jax.experimental.pallas import tpu as pltpu
from jax.sharding import Mesh
from jax.sharding import PartitionSpec as P


FS = ("ym", "yh")
TP = ("tz", "tc")
BLOCKS = ("pp", "tz", "tc")
EPS = 1e-06
T = 96
D = 1024
F32 = jnp.float32
BF16 = jnp.bfloat16
ROWS = 168


def lanes(shape):
    return lax.broadcasted_iota(jnp.int32, shape, len(shape) - 1)


def split3(v):
    hi = v.astype(BF16).astype(F32)
    mid = (v - hi).astype(BF16).astype(F32)
    low = v - hi - mid
    return hi, mid, low


def flag(where_ref, row, width=256):
    return where_ref[row : row + 1, :width] == 0


def permuted(v):
    group = lanes((v.shape[0], 128)) // 32
    out = []
    for h in range(2):
        for c in range(2):
            for p in range(2):
                block = None
                for g in range(4):
                    zz, m = g // 2, g % 2
                    n = (2 * p + zz) * 2 + c
                    moved = v[:, n * 128 : (n + 1) * 128]
                    turn = (64 * zz - 32 * m - 32 * h) % 128
                    if turn:
                        moved = pltpu.roll(moved, turn, 1)
                    block = moved if block is None else jnp.where(group == g, moved, block)
                out.append(block)
    return out


def pack_kernel(
    where_ref,
    micro_hbm,
    gate_hbm,
    value_hbm,
    step_hbm,
    out_hbm,
    taps_hbm,
    bias_hbm,
    decay_hbm,
    skip_hbm,
    gain_hbm,
    taps_w_hbm,
    taps_r_hbm,
    near_ref,
    away_ref,
    same_ref,
    other_ref,
    gain_out,
    taps_w_out,
    taps_r_out,
    *scratch,
):
    sources = (
        gate_hbm,
        value_hbm,
        out_hbm,
        step_hbm,
        taps_hbm,
        bias_hbm,
        decay_hbm,
        skip_hbm,
        gain_hbm,
        micro_hbm,
        taps_w_hbm,
        taps_r_hbm,
    )
    buffers, sems = (*scratch[:-1], taps_w_out, taps_r_out), scratch[-1]
    copies = [pltpu.make_async_copy(s, b, sems.at[i]) for i, (s, b) in enumerate(zip(sources, buffers))]
    for copy in copies:
        copy.start()
    for copy in copies:
        copy.wait()
    gate_ref, value_ref, out_ref, step_ref, taps_ref, bias_ref, decay_ref, skip_ref, gain_ref, micro_ref = buffers[:10]
    core = flag(where_ref, 1, 128)
    half = flag(where_ref, 0, 128)
    gate = jnp.concatenate(permuted(gate_ref[...].astype(F32)), axis=1).astype(BF16)
    value = jnp.concatenate(permuted(value_ref[...].astype(F32)), axis=1).astype(BF16)
    step = jnp.concatenate(permuted(step_ref[...].astype(F32)), axis=1)
    gain_out[...] = jnp.concatenate(permuted(gain_ref[...]), axis=1)
    blank = jnp.zeros((1, 64), F32)
    wide = lambda ref, k: jnp.broadcast_to(ref[:, k : k + 1], (1, 128))
    row_a = [taps_ref[k] for k in range(5) for _ in range(2)]
    row_a = jnp.concatenate(row_a + [wide(bias_ref, 0), wide(bias_ref, 1), blank, blank], axis=1)
    row_b = [wide(decay_ref, 0), wide(decay_ref, 1), wide(skip_ref, 0)] + [blank] * 10
    row_b = jnp.concatenate(row_b, axis=1)
    misc = jnp.concatenate([step, *split3(row_a), *split3(row_b)], axis=0).astype(BF16)
    out = permuted(out_ref[...].astype(F32))
    halves = []
    for h in range(2):
        first, second = out[4 * h : 4 * h + 2], out[4 * h + 2 : 4 * h + 4]
        own = [jnp.where(core, a, b) for a, b in zip(first, second)]
        far = [jnp.where(core, b, a) for a, b in zip(first, second)]
        halves.append(own + far)
    for ref, pair in ((same_ref, zip(*halves)), (other_ref, zip(*halves[::-1]))):
        part = jnp.concatenate([jnp.where(half, a, b) for a, b in pair], axis=1)
        ref[0:64] = gate
        ref[64:128] = value
        ref[128:160] = jnp.concatenate([part[0:32], part[32:64]], axis=1).astype(BF16)
        ref[160:168] = misc
    first = flag(where_ref, 4, 32)
    micro = [micro_ref[m].astype(F32) for m in range(2)]
    near_ref[...] = jnp.where(first, micro[0], micro[1]).astype(BF16)
    away_ref[...] = jnp.where(first, micro[1], micro[0]).astype(BF16)


def block_kernel(where_ref, r0_ref, r1_ref, r2_ref, r3_ref, send_ref):
    y = 2 * where_ref[4:5, :128] + where_ref[0:1, :128]
    group = lanes((24, 128)) // 32
    blank = jnp.zeros((24, 96), F32)
    block = jnp.zeros((24, 128), F32)
    for bits, ref in enumerate((r0_ref, r1_ref, r2_ref, r3_ref)):
        wide = jnp.concatenate([ref[...].astype(F32), blank], axis=1)
        for k in range(4):
            moved = wide if k == 0 else pltpu.roll(wide, 32 * k, 1)
            block = jnp.where((group == k) & ((y ^ bits) == group), moved, block)
    block = block.astype(BF16)
    for peer in range(32):
        send_ref[peer] = block


def nt_dot(a, b):
    return lax.dot_general(a, b, (((1,), (1,)), ((), ())), preferred_element_type=F32)


def nn_dot(a, b):
    return lax.dot_general(a, b, (((1,), (0,)), ((), ())), preferred_element_type=F32)


def silu(v):
    return v * jax.nn.sigmoid(v)


def section_body(quarters, weight_refs, write_ref, read_ref, gain_ref, taps_refs, own_ref, far_ref, pad_ref):
    low = lanes((T, 128)) < 64
    total = None
    for pair in quarters:
        for q in pair:
            sq = q * q
            sq = sq[:, :128] + sq[:, 128:]
            total = sq if total is None else total + sq
    scale = lax.rsqrt(jnp.sum(total, axis=1, keepdims=True) * (1.0 / D) + EPS)
    blocks = []
    for h in range(2):
        for c in range(2):
            n = (2 * h + c) * 256
            blocks.append((quarters[h][c] * scale * gain_ref[:, n : n + 256]).astype(BF16))
    normed = jnp.concatenate(blocks, axis=1)

    step_rows = jnp.concatenate([w[160:168].astype(F32)[0:2] for w in weight_refs], axis=0)
    step_raw = nt_dot(step_rows.astype(BF16), normed)
    small = []
    for w in weight_refs:
        misc = w[160:168].astype(F32)
        small.append((misc[2:3] + misc[3:4] + misc[4:5], misc[5:6] + misc[6:7] + misc[7:8]))
    bias = jnp.concatenate([s[0][:, 640 + 128 * d : 640 + 128 * d + T] for s in small for d in range(2)], axis=0)
    decay = jnp.concatenate([s[1][:, 128 * d : 128 * d + T] for s in small for d in range(2)], axis=0)
    raw = step_raw + bias
    dt = jnp.maximum(raw, 0.0) + jnp.log1p(jnp.exp(-jnp.abs(raw)))
    log_decay = dt * (-jnp.exp(decay))
    parts = [s.astype(BF16) for s in split3(log_decay)]
    row_id = lax.broadcasted_iota(jnp.int32, (T, T), 0)
    col_id = lax.broadcasted_iota(jnp.int32, (T, T), 1)
    upto = (row_id <= col_id).astype(F32).astype(BF16)
    since = (row_id >= col_id).astype(F32).astype(BF16)
    fwd_all = (nn_dot(parts[0], upto) + nn_dot(parts[1], upto)) + nn_dot(parts[2], upto)
    bwd_all = (nn_dot(parts[0], since) + nn_dot(parts[1], since)) + nn_dot(parts[2], since)
    odd = lax.broadcasted_iota(jnp.int32, (8, T), 0) % 2 == 1
    cum = jnp.where(odd, bwd_all, fwd_all)
    cum_pad = jnp.concatenate([cum, jnp.zeros((8, 128 - T), F32)], axis=1)
    cum_cols = cum_pad.T[:T]

    wr_rows = [
        jnp.concatenate([r[n * 128 + y * 32 : n * 128 + y * 32 + 32] for r in (write_ref, read_ref)], axis=1)
        for h in range(2)
        for c in range(2)
        for n in (c, 2 + c, 4 + c, 6 + c)
        for y in (h, 2 + h)
    ]
    wr = nn_dot(normed, jnp.concatenate(wr_rows, axis=0))
    pad_ref[0:8, 0:512] = jnp.zeros((8, 512), F32)
    pad_ref[8 + T : 16 + T, 0:512] = jnp.zeros((8, 512), F32)
    for i in range(2):
        pair = weight_refs[2 * i : 2 * i + 2]
        rows = jnp.concatenate([w[k * 64 : k * 64 + 64] for k in range(2) for w in pair], axis=0)
        gate_value = nt_dot(normed, rows).astype(BF16).astype(F32)
        pad_ref[8 : 8 + T, 512 + 128 * i : 640 + 128 * i] = gate_value[:, :128]
        pad_ref[8 : 8 + T, 128 * i : 128 * i + 128] = gate_value[:, 128:]
    pad_ref[8 : 8 + T, 256:512] = wr.astype(BF16).astype(F32)
    low_row = lanes((1, 128)) < 64
    acts = []
    for g in range(4):
        span = slice(g * 128, (g + 1) * 128)
        acc = None
        for k in range(5):
            if g < 2:
                tap = jnp.where(low_row, *[small[2 * g + e][0][:, k * 128 : (k + 1) * 128] for e in range(2)])
            else:
                tap = taps_refs[g - 2][k]
            term = pad_ref[6 + k : 6 + k + T, span] * tap
            acc = term if acc is None else acc + term
        acts.append(silu(acc).astype(BF16))
    scores = nt_dot(acts[3], acts[2])
    lower = row_id >= col_id
    diagonal = row_id == col_id
    pairs = []
    for i in range(2):
        high = []
        for j in (2 * i, 2 * i + 1):
            fc = cum_cols[:, 2 * j : 2 * j + 1]
            bc = cum_cols[:, 2 * j + 1 : 2 * j + 2]
            fr = cum[2 * j : 2 * j + 1]
            br = cum[2 * j + 1 : 2 * j + 2]
            d0 = dt[2 * j : 2 * j + 1]
            d1 = dt[2 * j + 1 : 2 * j + 2]
            mix = jnp.exp(jnp.where(lower, fc - fr, bc - br)) * jnp.where(lower, d0, d1)
            mix = mix + jnp.where(diagonal, d1, 0.0)
            combined = scores * mix
            high.append(combined.astype(BF16))
        y = nn_dot(jnp.concatenate(high, axis=0), acts[i])
        skip = jnp.where(low_row, *[small[2 * i + e][1][:, 256:384] for e in range(2)])
        y = jnp.where(low, y[:T], y[T:]) + skip * acts[i].astype(F32)
        gate = pad_ref[8 : 8 + T, 512 + 128 * i : 640 + 128 * i]
        pairs.append((y * silu(gate)).astype(BF16))
    gated_all = jnp.concatenate(pairs, axis=1)
    for side, ref in ((0, own_ref), (1, far_ref)):
        weight = jnp.concatenate(
            [
                w[128:160, 512 * r + 256 * side : 512 * r + 256 * side + 256]
                for w in weight_refs
                for r in range(2)
            ],
            axis=0,
        )
        ref[...] = nn_dot(gated_all, weight).astype(ref.dtype)


def entry_section_kernel(where_ref, recv_ref, *refs):
    *rest, quarter_out, own_ref, far_ref, pad_ref, quarter_ref = refs
    tokens = [
        jnp.concatenate([recv_ref[x * 8 + n].astype(F32) for x in range(4)], axis=0) for n in range(8)
    ]
    blocks = permuted(jnp.concatenate(tokens, axis=1))
    for q in range(4):
        quarter_ref[q] = jnp.concatenate(blocks[2 * q : 2 * q + 2], axis=1)
    quarters = [[quarter_ref[2 * h + c] for c in range(2)] for h in range(2)]
    half, core = flag(where_ref, 0), flag(where_ref, 1)
    mine = jnp.where(half, jnp.where(core, *quarters[0]), jnp.where(core, *quarters[1]))
    quarter_out[...] = mine.astype(BF16)
    section_body(quarters, rest[0:4], *rest[4:7], rest[7:9], own_ref, far_ref, pad_ref)


def relay_section_kernel(where_ref, a_ref, b_ref, c_ref, d_ref, *refs):
    *rest, own_ref, far_ref, pad_ref = refs
    half, core = flag(where_ref, 0), flag(where_ref, 1)
    a, b, c, d = [r[...].astype(F32) for r in (a_ref, b_ref, c_ref, d_ref)]
    own0, own1 = jnp.where(half, a, c), jnp.where(half, c, a)
    far0, far1 = jnp.where(half, b, d), jnp.where(half, d, b)
    quarters = [
        [jnp.where(core, own0, far0), jnp.where(core, far0, own0)],
        [jnp.where(core, own1, far1), jnp.where(core, far1, own1)],
    ]
    section_body(quarters, rest[0:4], *rest[4:7], rest[7:9], own_ref, far_ref, pad_ref)


def exit_pack_kernel(where_ref, mine_ref, m0_ref, m1_ref, m2_ref, m3_ref, send_ref):
    branch = (m0_ref[...].astype(F32) + m1_ref[...].astype(F32)) + (m2_ref[...].astype(F32) + m3_ref[...].astype(F32))
    branch = branch.astype(BF16).astype(F32)
    final = (mine_ref[...].astype(F32) + 0.5 * branch).astype(BF16).astype(F32)
    squares = final * final
    squares = jnp.sum(squares[:, :128] + squares[:, 128:], axis=1, keepdims=True)
    squares = jnp.broadcast_to(squares, (T, 128))
    own = jnp.where(flag(where_ref, 2, 128), final[:, :128], final[:, 128:])
    own = jnp.where(flag(where_ref, 3, 128), own, pltpu.roll(own, 64, 1))
    turned = {d: own if d == 0 else pltpu.roll(own, (32 * d) % 128, 1) for d in (-1, 0, 1, 2, 3)}
    lane = lanes((6, 128))
    group = lane // 32
    spot = lane % 32 == lax.broadcasted_iota(jnp.int32, (6, 128), 0)
    for x in range(4):
        rows = [slice(x * 24 + k * 6, x * 24 + k * 6 + 6) for k in range(4)]
        total = squares[rows[0]]
        for k in range(1, 4):
            total = jnp.where(group == k, squares[rows[k]], total)
        total = jnp.sum(jnp.where(spot, total, 0.0), axis=0, keepdims=True)
        parts = split3(total)
        for m in range(2):
            block = turned[-m][rows[0]]
            for k in range(1, 4):
                block = jnp.where(group == k, turned[k - m][rows[k]], block)
            message = jnp.concatenate([block, parts[0], parts[1]], axis=0).astype(BF16)
            for peer in range(4):
                send_ref[(x * 2 + m) * 4 + peer] = message


def exit_unpack_kernel(where_ref, recv_ref, out_ref):
    half, core = flag(where_ref, 0, 128), flag(where_ref, 1, 128)
    lane = lanes((8, 128))
    spot = lane % 32 == lax.broadcasted_iota(jnp.int32, (8, 128), 0)
    same_group = (
        lax.broadcasted_iota(jnp.int32, (128, 128), 0) // 32 == lanes((128, 128)) // 32
    ).astype(F32).astype(BF16)
    parts = []
    for m in range(2):
        first = (6 + m) * 4
        sums = [recv_ref[first + i].astype(F32) for i in range(4)]
        total = (sums[0][6:7] + sums[0][7:8]) + (sums[1][6:7] + sums[1][7:8])
        total = total + ((sums[2][6:7] + sums[2][7:8]) + (sums[3][6:7] + sums[3][7:8]))
        parts += split3(jnp.where(spot, jnp.broadcast_to(total, (8, 128)), 0.0))
    spread = nn_dot(jnp.concatenate(parts, axis=0).astype(BF16), same_group)
    for m in range(2):
        total = (spread[24 * m : 24 * m + 8] + spread[24 * m + 8 : 24 * m + 16]) + spread[24 * m + 16 : 24 * m + 24]
        blocks = [recv_ref[(6 + m) * 4 + i].astype(F32) for i in range(4)]
        block = jnp.where(half, jnp.where(core, *blocks[:2]), jnp.where(core, *blocks[2:]))
        block = block * lax.rsqrt(total * (1.0 / D) + EPS)
        rows = [block if k == 0 else pltpu.roll(block, 128 - 32 * k, 1) for k in range(4)]
        out_ref[m] = jnp.concatenate([r[:6, :32] for r in rows], axis=0).astype(BF16)


VMEM_SPEC = pl.BlockSpec(memory_space=pltpu.VMEM)


def call_kernel(kernel, out_shape, count, scratch=()):
    return pl.pallas_call(
        kernel,
        out_shape=out_shape,
        in_specs=[VMEM_SPEC] + [VMEM_SPEC] * count,
        out_specs=[VMEM_SPEC] * len(out_shape),
        scratch_shapes=scratch,
        compiler_params=pltpu.CompilerParams(vmem_limit_bytes=24 * 1024 * 1024),
    )


def flip(v, axes, bits):
    size = lax.axis_size(axes)
    return lax.ppermute(v, axes, [(i, i ^ bits) for i in range(size)])


def sum_pairs(active, sections, bits):
    pairs = []
    for i in range(sections):
        for z in range(4):
            for c in range(2):
                target = 2 * (z ^ bits) + c if i == active else 2 * z + 1 - c
                pairs.append((8 * i + 2 * z + c, 8 * i + target))
    return pairs


def per_device(
    micro_in,
    norm_gain,
    proj_gate,
    proj_value,
    proj_write,
    proj_read,
    proj_step,
    step_bias,
    decay_log,
    skip_gain,
    conv_value,
    conv_write,
    conv_read,
    proj_out,
):
    sections = lax.axis_size("pp")
    half = lax.axis_index("yh")
    micro = lax.axis_index("ym")
    core = lax.axis_index("tc")
    zpos = lax.axis_index("tz")
    where = jnp.stack([half, core, zpos // 2, zpos % 2, micro]).astype(jnp.int32)
    where = jnp.broadcast_to(where[:, None], (5, 256))

    shape = jax.ShapeDtypeStruct
    raw = (
        micro_in,
        proj_gate[0, :, 0, 0, :].T,
        proj_value[0, :, 0, 0, :].T,
        proj_step[0, :, :, 0, 0].T,
        proj_out[0, 0, 0],
        conv_value.reshape(5, 1, 64),
        step_bias.reshape(1, 2),
        decay_log.reshape(1, 2),
        skip_gain.reshape(1, 1),
        norm_gain,
        conv_write.reshape(5, 1, 128),
        conv_read.reshape(5, 1, 128),
    )
    order = (1, 2, 4, 3, 5, 6, 7, 8, 9, 0)
    near, away, same, other, gain, taps_w, taps_r = pl.pallas_call(
        pack_kernel,
        out_shape=[
            shape((T // 4, 32), BF16),
            shape((T // 4, 32), BF16),
            shape((ROWS, D), BF16),
            shape((ROWS, D), BF16),
            shape((1, D), F32),
            shape((5, 1, 128), F32),
            shape((5, 1, 128), F32),
        ],
        in_specs=[VMEM_SPEC] + [pl.BlockSpec(memory_space=pltpu.HBM)] * len(raw),
        out_specs=[VMEM_SPEC] * 7,
        scratch_shapes=[pltpu.VMEM(raw[i].shape, raw[i].dtype) for i in order]
        + [pltpu.SemaphoreType.DMA((len(raw),))],
        compiler_params=pltpu.CompilerParams(vmem_limit_bytes=24 * 1024 * 1024),
    )(where, *[pltpu.with_memory_space_constraint(v, pltpu.HBM) if i != 8 else v for i, v in enumerate(raw)])
    r1 = flip(near, FS, 1)
    r2 = flip(away, FS, 2)
    r3 = flip(away, FS, 3)
    w1 = flip(other, FS, 1)
    w2 = flip(same, FS, 2)
    w3 = flip(other, FS, 3)
    (send,) = call_kernel(block_kernel, [shape((32, T // 4, 128), BF16)], 4)(where, near, r1, r2, r3)
    recv = lax.all_to_all(send, BLOCKS, 0, 0)

    params = (same, w1, w2, w3, proj_write[0, :, 0, :], proj_read[0, :, 0, :], gain, taps_w, taps_r)
    quarter = shape((T, 256), BF16)
    outs = [shape((T, 256), F32), quarter]
    pad = pltpu.VMEM((T + 16, 768), F32)
    mine, own, far = call_kernel(
        entry_section_kernel, [quarter, *outs], 10, [pad, pltpu.VMEM((4, T, 256), F32)]
    )(where, recv, *params)
    hop = [(i, (i + 1) % sections) for i in range(sections)]
    hop_flip = [(2 * i + h, 2 * j + 1 - h) for i, j in hop for h in range(2)]
    for s in range(sections):
        got = flip(far, "tc", 1)
        mixed = (own + got.astype(F32)).astype(BF16)
        others = []
        for d in (1, 2, 3):
            others.append(lax.ppermute(mixed, ("pp", "tz", "tc"), sum_pairs(s, sections, d)))
        if s + 1 == sections:
            break
        r1, r2, r3 = [v.astype(F32) for v in others]
        branch = ((mixed.astype(F32) + r1) + (r2 + r3)).astype(BF16).astype(F32)
        produced = (mine.astype(F32) + 0.5 * branch).astype(BF16)
        a = lax.ppermute(produced, "pp", hop)
        c = lax.ppermute(produced, ("pp", "yh"), hop_flip)
        b = flip(a, "tc", 1)
        d = flip(c, "tc", 1)
        mine = a
        own, far = call_kernel(relay_section_kernel, outs, 13, [pad])(where, a, b, c, d, *params)

    (send,) = call_kernel(exit_pack_kernel, [shape((32, 8, 128), BF16)], 5)(where, mine, mixed, *others)
    recv = lax.all_to_all(send, ("pp", "ym", "yh", "tc"), 0, 0)
    (result,) = call_kernel(exit_unpack_kernel, [shape((2, T // sections, 32), BF16)], 1)(where, recv)
    return result


def solution(mesh):
    split = Mesh(
        mesh.devices.reshape(mesh.shape["pp"], 2, 2, 4, 2), ("pp", "ym", "yh", "tz", "tc")
    )
    in_specs = (
        P(None, "pp", TP + FS),
        P("pp", None),
        P("pp", None, TP, FS, None),
        P("pp", None, TP, FS, None),
        P("pp", None, TP, None),
        P("pp", None, TP, None),
        P("pp", None, None, TP, FS),
        P("pp", None, TP, FS),
        P("pp", None, TP, FS),
        P("pp", TP, FS),
        P("pp", None, TP, FS, None),
        P("pp", None, TP, None),
        P("pp", None, TP, None),
        P("pp", TP, FS, None, None),
    )
    out_specs = P(None, "pp", TP + FS)
    return jax.shard_map(
        per_device, mesh=split, in_specs=in_specs, out_specs=out_specs, check_vma=False
    )
```

profile of v0, /device:TPU:1, one launch (start us, length us, event | category | flops | bytes accessed | tf_op | source)
XLA Modules:
  0.0 113.4 jit_solution(12996026428587416840)
XLA Ops:
  0.8 1.5 %shard_map.136 = (bf16[24,32]{1,0:T(8,128)(2,1)S(1)}, bf16[24,32]{1,0:T(8,128)(2,1)S(1)}, bf16[168,1024]{1,0:T(8,128)(2,1)S(1)}, bf16[168,1024]{1,0:T(8,128)(2,1...) custom-call(s32[5,256]{1,0:T(8,128)S(1)} %broadcast_in_dim.2.where_ref, ...), custom_call_target="tpu_custom_call" | custom-call | tf_op jit(solution)/shard_map/pallas_call | solution.py:412
  2.4 3.6 %collective-permute-start.5 = (bf16[168,1024]{1,0:T(8,128)(2,1)S(1)}, bf16[168,1024]{1,0:T(8,128)(2,1)S(1)}, u32[]{:S(2)}, u32[]{:S(2)}) collective-permute-start(bf16[168,1024]{1,0:T(8,128)(2,1)S(1)} %get-tuple-element.24), channel_id=1, source_target_pairs={{0,24},{8,16},{16,8},{24,0},{1,25},{9,17},{17,9},{25,1},{2,26},{10... | collective-permute-start | bytes 1032200 | tf_op jit(solution)/shard_map/ppermute | solution.py:359
  6.0 1.3 %collective-permute-start.4 = (bf16[168,1024]{1,0:T(8,128)(2,1)S(1)}, bf16[168,1024]{1,0:T(8,128)(2,1)S(1)}, u32[]{:S(2)}, u32[]{:S(2)}) collective-permute-start(bf16[168,1024]{1,0:T(8,128)(2,1)S(1)} %get-tuple-element.23.refs_0_), channel_id=1, source_target_pairs={{0,16},{8,24},{16,0},{24,8},{1,17},{9,25},{17,1},{25,9},{2,18},{10... | collective-permute-start | bytes 1032200 | tf_op jit(solution)/shard_map/ppermute | solution.py:359
  7.3 0.2 collective-permute-start
  7.5 2.4 %collective-permute-start.2 = (bf16[24,32]{1,0:T(8,128)(2,1)S(1)}, bf16[24,32]{1,0:T(8,128)(2,1)S(1)}, u32[]{:S(2)}, u32[]{:S(2)}) collective-permute-start(bf16[24,32]{1,0:T(8,128)(2,1)S(1)} %get-tuple-element.22), channel_id=1, source_target_pairs={{0,24},{8,16},{16,8},{24,0},{1,25},{9,17},{17,9},{25,1},{2,26},{10... | collective-permute-start | bytes 4616 | tf_op jit(solution)/shard_map/ppermute | solution.py:359
  9.9 12.3 %collective-permute-done.r1_ref = bf16[24,32]{1,0:T(8,128)(2,1)S(1)} collective-permute-done((bf16[24,32]{1,0:T(8,128)(2,1)S(1)}, bf16[24,32]{1,0:T(8,128)(2,1)S(1)}, u32[]{:S(2)}, u32[]{:S(2)}) %collective-permute-start) | collective-permute-done | bytes 1568 | tf_op jit(solution)/shard_map/ppermute | solution.py:359
  22.2 0.3 collective-permute-start.1
  22.5 3.6 %collective-permute-done.1.r2_ref = bf16[24,32]{1,0:T(8,128)(2,1)S(1)} collective-permute-done((bf16[24,32]{1,0:T(8,128)(2,1)S(1)}, bf16[24,32]{1,0:T(8,128)(2,1)S(1)}, u32[]{:S(2)}, u32[]{:S(2)}) %collective-permute-start.1) | collective-permute-done | bytes 1568 | tf_op jit(solution)/shard_map/ppermute | solution.py:359
  26.3 19.0 %all_to_all.10.recv_ref = bf16[32,24,128]{2,1,0:T(8,128)(2,1)S(1)} all-to-all(bf16[32,24,128]{2,1,0:T(8,128)(2,1)S(1)} %shard_map.137), channel_id=1, replica_groups=mesh['pp'=4,'ym'=2,'yh'=2,'tz'=4,'tc'=2] {'pp','tz','tc'}, dimensions={0} | all-to-all | bytes 393216 | tf_op jit(solution)/shard_map/all_to_all | solution.py:436
  45.3 1.6 %shard_map.138 = (bf16[96,256]{1,0:T(8,128)(2,1)S(1)}, f32[96,256]{1,0:T(8,128)S(1)}, bf16[96,256]{1,0:T(8,128)(2,1)S(1)}) custom-call(s32[5,256]{1,0:T(8,128)S(1)} %broadcast_in_dim.2.where_ref, bf16[32,24,128]{2,1,0:T(8,128)(2,1)S(1)} %all_to_all.10.recv_ref, bf16[168,1024]{1,0:T(8,128)(2,1)S(1)} %get-tuple-element.23.refs_0_, ...), custom_call_target="tpu_custom_call" | custom-call | tf_op jit(solution)/shard_map/pallas_call | solution.py:442
  46.8 0.4 collective-permute-start.6
  47.2 0.9 collective-permute-done.6
  48.2 1.0 collective-permute-start.9
  49.2 1.1 collective-permute-start.8
  50.3 1.2 %collective-permute-start.7 = (bf16[96,256]{1,0:T(8,128)(2,1)S(1)}, bf16[96,256]{1,0:T(8,128)(2,1)S(1)}, u32[]{:S(2)}, u32[]{:S(2)}) collective-permute-start(bf16[96,256]{1,0:T(8,128)(2,1)S(1)} %add_convert_fusion.9), channel_id=1, source_target_pairs={{0,2},{1,3},{2,0},{3,1},{4,6},{5,7},{6,4},{7,5},{32,33},{33,32},{3... | collective-permute-start | bytes 147464 | tf_op jit(solution)/shard_map/ppermute | solution.py:452
  51.5 0.9 collective-permute-done.9
  52.4 1.3 %collective-permute-done.8 = bf16[96,256]{1,0:T(8,128)(2,1)S(1)} collective-permute-done((bf16[96,256]{1,0:T(8,128)(2,1)S(1)}, bf16[96,256]{1,0:T(8,128)(2,1)S(1)}, u32[]{:S(2)}, u32[]{:S(2)}) %collective-permute-start.8) | collective-permute-done | bytes 49184 | tf_op jit(solution)/shard_map/ppermute | solution.py:452
  53.9 5.0 %collective-permute-done.12.c_ref = bf16[96,256]{1,0:T(8,128)(2,1)S(1)} collective-permute-done((bf16[96,256]{1,0:T(8,128)(2,1)S(1)}, bf16[96,256]{1,0:T(8,128)(2,1)S(1)}, u32[]{:S(2)}, u32[]{:S(2)}) %collective-permute-start.12) | collective-permute-done | bytes 49184 | tf_op jit(solution)/shard_map/ppermute | solution.py:459
  58.9 2.8 %collective-permute-start.13 = (bf16[96,256]{1,0:T(8,128)(2,1)S(1)}, bf16[96,256]{1,0:T(8,128)(2,1)S(1)}, u32[]{:S(2)}, u32[]{:S(2)}) collective-permute-start(bf16[96,256]{1,0:T(8,128)(2,1)S(1)} %collective-permute-done.12.c_ref), channel_id=1, source_target_pairs={{0,1},{1,0},{2,3},{3,2},{4,5},{5,4},{6,7},{7,6},{8,9},{9,8},{10,11... | collective-permute-start | bytes 147464 | tf_op jit(solution)/shard_map/ppermute | solution.py:359
  61.7 0.9 collective-permute-done.13.d_ref
  62.6 0.4 collective-permute-done.11.b_ref
  62.9 1.4 %shard_map.139 = (f32[96,256]{1,0:T(8,128)S(1)}, bf16[96,256]{1,0:T(8,128)(2,1)S(1)}) custom-call(s32[5,256]{1,0:T(8,128)S(1)} %broadcast_in_dim.2.where_ref, bf16[96,256]{1,0:T(8,128)(2,1)S(1)} %collective-permute-done.10.a_ref, bf16[96,256]{1,0:T(8,128)(2,1)S(1)} %collective-permute-done.11.b_ref, bf16[96,256]{1,0:T(8,128)(2,1)S(1)} %collective-permute-done.12.c_ref, ...), custom_call_target="tpu_custom_call" | custom-call | tf_op jit(solution)/shard_map/pallas_call | solution.py:463
  64.4 0.2 collective-permute-start.14
  64.6 1.1 collective-permute-done.14
  65.7 0.2 collective-permute-start.17
  65.9 0.3 collective-permute-start.16
  66.3 0.2 collective-permute-start.15
  66.4 0.6 collective-permute-done.17
  67.0 0.2 collective-permute-done.16
  67.2 0.3 collective-permute-done.15
  67.6 3.0 %collective-permute-start.20 = (bf16[96,256]{1,0:T(8,128)(2,1)S(1)}, bf16[96,256]{1,0:T(8,128)(2,1)S(1)}, u32[]{:S(2)}, u32[]{:S(2)}) collective-permute-start(bf16[96,256]{1,0:T(8,128)(2,1)S(1)} %add_convert_fusion.4), channel_id=1, source_target_pairs={{0,40},{8,32},{32,72},{40,64},{64,104},{72,96},{96,8},{104,0},{1,4... | collective-permute-start | bytes 147464 | tf_op jit(solution)/shard_map/ppermute | solution.py:459
  70.6 2.1 %collective-permute-done.20.c_ref = bf16[96,256]{1,0:T(8,128)(2,1)S(1)} collective-permute-done((bf16[96,256]{1,0:T(8,128)(2,1)S(1)}, bf16[96,256]{1,0:T(8,128)(2,1)S(1)}, u32[]{:S(2)}, u32[]{:S(2)}) %collective-permute-start.20) | collective-permute-done | bytes 49184 | tf_op jit(solution)/shard_map/ppermute | solution.py:459
  72.7 1.7 %collective-permute-start.21 = (bf16[96,256]{1,0:T(8,128)(2,1)S(1)}, bf16[96,256]{1,0:T(8,128)(2,1)S(1)}, u32[]{:S(2)}, u32[]{:S(2)}) collective-permute-start(bf16[96,256]{1,0:T(8,128)(2,1)S(1)} %collective-permute-done.20.c_ref), channel_id=1, source_target_pairs={{0,1},{1,0},{2,3},{3,2},{4,5},{5,4},{6,7},{7,6},{8,9},{9,8},{10,11... | collective-permute-start | bytes 147464 | tf_op jit(solution)/shard_map/ppermute | solution.py:359
  74.4 0.4 collective-permute-done.18.a_ref
  74.7 3.2 %collective-permute-start.19 = (bf16[96,256]{1,0:T(8,128)(2,1)S(1)}, bf16[96,256]{1,0:T(8,128)(2,1)S(1)}, u32[]{:S(2)}, u32[]{:S(2)}) collective-permute-start(bf16[96,256]{1,0:T(8,128)(2,1)S(1)} %collective-permute-done.18.a_ref), channel_id=1, source_target_pairs={{0,1},{1,0},{2,3},{3,2},{4,5},{5,4},{6,7},{7,6},{8,9},{9,8},{10,11... | collective-permute-start | bytes 147464 | tf_op jit(solution)/shard_map/ppermute | solution.py:359
  77.9 0.9 collective-permute-done.19.b_ref
  78.8 1.4 %shard_map.140 = (f32[96,256]{1,0:T(8,128)S(1)}, bf16[96,256]{1,0:T(8,128)(2,1)S(1)}) custom-call(s32[5,256]{1,0:T(8,128)S(1)} %broadcast_in_dim.2.where_ref, bf16[96,256]{1,0:T(8,128)(2,1)S(1)} %collective-permute-done.18.a_ref, bf16[96,256]{1,0:T(8,128)(2,1)S(1)} %collective-permute-done.19.b_ref, bf16[96,256]{1,0:T(8,128)(2,1)S(1)} %collective-permute-done.20.c_ref, ...), custom_call_target="tpu_custom_call" | custom-call | tf_op jit(solution)/shard_map/pallas_call | solution.py:463
  80.2 0.4 collective-permute-start.22
  80.6 0.9 collective-permute-done.22
  81.5 0.4 collective-permute-start.25
  82.0 0.2 collective-permute-start.24
  82.1 0.3 collective-permute-start.23
  82.5 0.4 collective-permute-done.25
  82.8 0.3 collective-permute-done.24
  83.2 0.2 collective-permute-done.23
  83.4 0.3 collective-permute-start.28
  83.7 2.9 %collective-permute-start.26 = (bf16[96,256]{1,0:T(8,128)(2,1)S(1)}, bf16[96,256]{1,0:T(8,128)(2,1)S(1)}, u32[]{:S(2)}, u32[]{:S(2)}) collective-permute-start(bf16[96,256]{1,0:T(8,128)(2,1)S(1)} %add_convert_fusion.1), channel_id=1, source_target_pairs={{0,32},{32,64},{64,96},{96,0},{1,33},{33,65},{65,97},{97,1},{2,34}... | collective-permute-start | bytes 147464 | tf_op jit(solution)/shard_map/ppermute | solution.py:458
  86.6 2.1 %collective-permute-done.28.c_ref = bf16[96,256]{1,0:T(8,128)(2,1)S(1)} collective-permute-done((bf16[96,256]{1,0:T(8,128)(2,1)S(1)}, bf16[96,256]{1,0:T(8,128)(2,1)S(1)}, u32[]{:S(2)}, u32[]{:S(2)}) %collective-permute-start.28) | collective-permute-done | bytes 49184 | tf_op jit(solution)/shard_map/ppermute | solution.py:459
  88.7 1.7 %collective-permute-start.29 = (bf16[96,256]{1,0:T(8,128)(2,1)S(1)}, bf16[96,256]{1,0:T(8,128)(2,1)S(1)}, u32[]{:S(2)}, u32[]{:S(2)}) collective-permute-start(bf16[96,256]{1,0:T(8,128)(2,1)S(1)} %collective-permute-done.28.c_ref), channel_id=1, source_target_pairs={{0,1},{1,0},{2,3},{3,2},{4,5},{5,4},{6,7},{7,6},{8,9},{9,8},{10,11... | collective-permute-start | bytes 147464 | tf_op jit(solution)/shard_map/ppermute | solution.py:359
  90.4 0.3 collective-permute-start.27
  90.7 0.6 collective-permute-done.29.d_ref
  91.3 0.4 collective-permute-done.27.b_ref
  91.7 1.4 %shard_map.141 = (f32[96,256]{1,0:T(8,128)S(1)}, bf16[96,256]{1,0:T(8,128)(2,1)S(1)}) custom-call(s32[5,256]{1,0:T(8,128)S(1)} %broadcast_in_dim.2.where_ref, bf16[96,256]{1,0:T(8,128)(2,1)S(1)} %collective-permute-done.26.a_ref.mine_ref, bf16[96,256]{1,0:T(8,128)(2,1)S(1)} %collective-permute-done.27.b_ref, ...), custom_call_target="tpu_custom_call" | custom-call | tf_op jit(solution)/shard_map/pallas_call | solution.py:463
  93.1 0.3 collective-permute-start.30
  93.5 1.0 collective-permute-done.30
  94.4 0.3 collective-permute-start.33
  94.8 0.2 collective-permute-start.32
  95.0 0.3 collective-permute-start.31
  95.3 0.5 collective-permute-done.33.m3_ref
  95.7 0.3 collective-permute-done.32.m2_ref
  96.0 0.2 collective-permute-done.31.m1_ref
  96.3 0.2 shard_map.142
  96.5 16.1 %all_to_all.11.recv_ref = bf16[32,8,128]{2,1,0:T(8,128)(2,1)S(1)} all-to-all(bf16[32,8,128]{2,1,0:T(8,128)(2,1)S(1)} %shard_map.142), channel_id=1, replica_groups=mesh['pp'=4,'ym'=2,'yh'=2,'tz'=4,'tc'=2] {'pp','ym','yh','tc'}, dimensions={0} | all-to-all | bytes 131072 | tf_op jit(solution)/shard_map/all_to_all | solution.py:466
  112.6 0.8 shard_map.143
  (27 shorter events, 0.6 us)
Async XLA Ops:
  2.4 42.9 %collective-permute-start.5 = (bf16[168,1024]{1,0:T(8,128)(2,1)S(1)}, bf16[168,1024]{1,0:T(8,128)(2,1)S(1)}, u32[]{:S(2)}, u32[]{:S(2)}) collective-permute-start(bf16[168,1024]{1,0:T(8,128)(2,1)S(1)} %get-tuple-element.24), channel_id=1, source_target_pairs={{0,24},{8,16},{16,8},{24,0},{1,25},{9,17},{17,9},{25,1},{2,26},{10... | collective-permute-start | bytes 1032200 | tf_op jit(solution)/shard_map/ppermute | solution.py:359
  6.0 39.3 %collective-permute-start.3 = (bf16[168,1024]{1,0:T(8,128)(2,1)S(1)}, bf16[168,1024]{1,0:T(8,128)(2,1)S(1)}, u32[]{:S(2)}, u32[]{:S(2)}) collective-permute-start(bf16[168,1024]{1,0:T(8,128)(2,1)S(1)} %get-tuple-element.24), channel_id=1, source_target_pairs={{0,8},{8,0},{16,24},{24,16},{1,9},{9,1},{17,25},{25,17},{2,10},{10... | collective-permute-start | bytes 1032200 | tf_op jit(solution)/shard_map/ppermute | solution.py:359
  6.0 39.3 %collective-permute-start.4 = (bf16[168,1024]{1,0:T(8,128)(2,1)S(1)}, bf16[168,1024]{1,0:T(8,128)(2,1)S(1)}, u32[]{:S(2)}, u32[]{:S(2)}) collective-permute-start(bf16[168,1024]{1,0:T(8,128)(2,1)S(1)} %get-tuple-element.23.refs_0_), channel_id=1, source_target_pairs={{0,16},{8,24},{16,0},{24,8},{1,17},{9,25},{17,1},{25,9},{2,18},{10... | collective-permute-start | bytes 1032200 | tf_op jit(solution)/shard_map/ppermute | solution.py:359
  7.3 14.9 %collective-permute-start = (bf16[24,32]{1,0:T(8,128)(2,1)S(1)}, bf16[24,32]{1,0:T(8,128)(2,1)S(1)}, u32[]{:S(2)}, u32[]{:S(2)}) collective-permute-start(bf16[24,32]{1,0:T(8,128)(2,1)S(1)} %get-tuple-element.21.r0_ref), channel_id=1, source_target_pairs={{0,8},{8,0},{16,24},{24,16},{1,9},{9,1},{17,25},{25,17},{2,10},{10... | collective-permute-start | bytes 4616 | tf_op jit(solution)/shard_map/ppermute | solution.py:359
  7.5 37.8 %copy-start = (bf16[1,1024,1,128]{3,1,2,0:T(8,128)(2,1)S(1)}, bf16[1,1024,1,128]{3,1,2,0:T(8,128)(2,1)}, u32[]{:S(2)}) copy-start(bf16[1,1024,1,128]{3,1,2,0:T(8,128)(2,1)} %param.18) | copy-start | bytes 786436
  7.5 37.8 %copy-start.1 = (bf16[1,1024,1,128]{3,1,2,0:T(8,128)(2,1)S(1)}, bf16[1,1024,1,128]{3,1,2,0:T(8,128)(2,1)}, u32[]{:S(2)}) copy-start(bf16[1,1024,1,128]{3,1,2,0:T(8,128)(2,1)} %param.19) | copy-start | bytes 786436
  7.5 15.1 %collective-permute-start.2 = (bf16[24,32]{1,0:T(8,128)(2,1)S(1)}, bf16[24,32]{1,0:T(8,128)(2,1)S(1)}, u32[]{:S(2)}, u32[]{:S(2)}) collective-permute-start(bf16[24,32]{1,0:T(8,128)(2,1)S(1)} %get-tuple-element.22), channel_id=1, source_target_pairs={{0,24},{8,16},{16,8},{24,0},{1,25},{9,17},{17,9},{25,1},{2,26},{10... | collective-permute-start | bytes 4616 | tf_op jit(solution)/shard_map/ppermute | solution.py:359
  22.2 4.0 %collective-permute-start.1 = (bf16[24,32]{1,0:T(8,128)(2,1)S(1)}, bf16[24,32]{1,0:T(8,128)(2,1)S(1)}, u32[]{:S(2)}, u32[]{:S(2)}) collective-permute-start(bf16[24,32]{1,0:T(8,128)(2,1)S(1)} %get-tuple-element.22), channel_id=1, source_target_pairs={{0,16},{8,24},{16,0},{24,8},{1,17},{9,25},{17,1},{25,9},{2,18},{10... | collective-permute-start | bytes 4616 | tf_op jit(solution)/shard_map/ppermute | solution.py:359
  46.8 1.3 %collective-permute-start.6 = (bf16[96,256]{1,0:T(8,128)(2,1)S(1)}, bf16[96,256]{1,0:T(8,128)(2,1)S(1)}, u32[]{:S(2)}, u32[]{:S(2)}) collective-permute-start(bf16[96,256]{1,0:T(8,128)(2,1)S(1)} %get-tuple-element.30), channel_id=1, source_target_pairs={{0,1},{1,0},{2,3},{3,2},{4,5},{5,4},{6,7},{7,6},{8,9},{9,8},{10,11... | collective-permute-start | bytes 147464 | tf_op jit(solution)/shard_map/ppermute | solution.py:359
  48.2 4.2 %collective-permute-start.9 = (bf16[96,256]{1,0:T(8,128)(2,1)S(1)}, bf16[96,256]{1,0:T(8,128)(2,1)S(1)}, u32[]{:S(2)}, u32[]{:S(2)}) collective-permute-start(bf16[96,256]{1,0:T(8,128)(2,1)S(1)} %add_convert_fusion.9), channel_id=1, source_target_pairs={{0,6},{1,7},{2,4},{3,5},{4,2},{5,3},{6,0},{7,1},{32,33},{33,32},{3... | collective-permute-start | bytes 147464 | tf_op jit(solution)/shard_map/ppermute | solution.py:452
  49.2 4.5 %collective-permute-start.8 = (bf16[96,256]{1,0:T(8,128)(2,1)S(1)}, bf16[96,256]{1,0:T(8,128)(2,1)S(1)}, u32[]{:S(2)}, u32[]{:S(2)}) collective-permute-start(bf16[96,256]{1,0:T(8,128)(2,1)S(1)} %add_convert_fusion.9), channel_id=1, source_target_pairs={{0,4},{1,5},{2,6},{3,7},{4,0},{5,1},{6,2},{7,3},{32,33},{33,32},{3... | collective-permute-start | bytes 147464 | tf_op jit(solution)/shard_map/ppermute | solution.py:452
  50.3 3.4 %collective-permute-start.7 = (bf16[96,256]{1,0:T(8,128)(2,1)S(1)}, bf16[96,256]{1,0:T(8,128)(2,1)S(1)}, u32[]{:S(2)}, u32[]{:S(2)}) collective-permute-start(bf16[96,256]{1,0:T(8,128)(2,1)S(1)} %add_convert_fusion.9), channel_id=1, source_target_pairs={{0,2},{1,3},{2,0},{3,1},{4,6},{5,7},{6,4},{7,5},{32,33},{33,32},{3... | collective-permute-start | bytes 147464 | tf_op jit(solution)/shard_map/ppermute | solution.py:452
  53.7 5.1 %collective-permute-start.12 = (bf16[96,256]{1,0:T(8,128)(2,1)S(1)}, bf16[96,256]{1,0:T(8,128)(2,1)S(1)}, u32[]{:S(2)}, u32[]{:S(2)}) collective-permute-start(bf16[96,256]{1,0:T(8,128)(2,1)S(1)} %add_convert_fusion.7), channel_id=1, source_target_pairs={{0,40},{8,32},{32,72},{40,64},{64,104},{72,96},{96,8},{104,0},{1,4... | collective-permute-start | bytes 147464 | tf_op jit(solution)/shard_map/ppermute | solution.py:459
  53.8 7.9 %collective-permute-start.10 = (bf16[96,256]{1,0:T(8,128)(2,1)S(1)}, bf16[96,256]{1,0:T(8,128)(2,1)S(1)}, u32[]{:S(2)}, u32[]{:S(2)}) collective-permute-start(bf16[96,256]{1,0:T(8,128)(2,1)S(1)} %add_convert_fusion.7), channel_id=1, source_target_pairs={{0,32},{32,64},{64,96},{96,0},{1,33},{33,65},{65,97},{97,1},{2,34}... | collective-permute-start | bytes 147464 | tf_op jit(solution)/shard_map/ppermute | solution.py:458
  58.9 3.7 %collective-permute-start.13 = (bf16[96,256]{1,0:T(8,128)(2,1)S(1)}, bf16[96,256]{1,0:T(8,128)(2,1)S(1)}, u32[]{:S(2)}, u32[]{:S(2)}) collective-permute-start(bf16[96,256]{1,0:T(8,128)(2,1)S(1)} %collective-permute-done.12.c_ref), channel_id=1, source_target_pairs={{0,1},{1,0},{2,3},{3,2},{4,5},{5,4},{6,7},{7,6},{8,9},{9,8},{10,11... | collective-permute-start | bytes 147464 | tf_op jit(solution)/shard_map/ppermute | solution.py:359
  61.7 1.2 %collective-permute-start.11 = (bf16[96,256]{1,0:T(8,128)(2,1)S(1)}, bf16[96,256]{1,0:T(8,128)(2,1)S(1)}, u32[]{:S(2)}, u32[]{:S(2)}) collective-permute-start(bf16[96,256]{1,0:T(8,128)(2,1)S(1)} %collective-permute-done.10.a_ref), channel_id=1, source_target_pairs={{0,1},{1,0},{2,3},{3,2},{4,5},{5,4},{6,7},{7,6},{8,9},{9,8},{10,11... | collective-permute-start | bytes 147464 | tf_op jit(solution)/shard_map/ppermute | solution.py:359
  64.4 1.3 %collective-permute-start.14 = (bf16[96,256]{1,0:T(8,128)(2,1)S(1)}, bf16[96,256]{1,0:T(8,128)(2,1)S(1)}, u32[]{:S(2)}, u32[]{:S(2)}) collective-permute-start(bf16[96,256]{1,0:T(8,128)(2,1)S(1)} %get-tuple-element.32), channel_id=1, source_target_pairs={{0,1},{1,0},{2,3},{3,2},{4,5},{5,4},{6,7},{7,6},{8,9},{9,8},{10,11... | collective-permute-start | bytes 147464 | tf_op jit(solution)/shard_map/ppermute | solution.py:359
  65.7 1.3 %collective-permute-start.17 = (bf16[96,256]{1,0:T(8,128)(2,1)S(1)}, bf16[96,256]{1,0:T(8,128)(2,1)S(1)}, u32[]{:S(2)}, u32[]{:S(2)}) collective-permute-start(bf16[96,256]{1,0:T(8,128)(2,1)S(1)} %add_convert_fusion.6), channel_id=1, source_target_pairs={{0,1},{1,0},{2,3},{3,2},{4,5},{5,4},{6,7},{7,6},{32,38},{33,39},{3... | collective-permute-start | bytes 147464 | tf_op jit(solution)/shard_map/ppermute | solution.py:452
  65.9 1.2 %collective-permute-start.16 = (bf16[96,256]{1,0:T(8,128)(2,1)S(1)}, bf16[96,256]{1,0:T(8,128)(2,1)S(1)}, u32[]{:S(2)}, u32[]{:S(2)}) collective-permute-start(bf16[96,256]{1,0:T(8,128)(2,1)S(1)} %add_convert_fusion.6), channel_id=1, source_target_pairs={{0,1},{1,0},{2,3},{3,2},{4,5},{5,4},{6,7},{7,6},{32,36},{33,37},{3... | collective-permute-start | bytes 147464 | tf_op jit(solution)/shard_map/ppermute | solution.py:452
  66.3 1.2 %collective-permute-start.15 = (bf16[96,256]{1,0:T(8,128)(2,1)S(1)}, bf16[96,256]{1,0:T(8,128)(2,1)S(1)}, u32[]{:S(2)}, u32[]{:S(2)}) collective-permute-start(bf16[96,256]{1,0:T(8,128)(2,1)S(1)} %add_convert_fusion.6), channel_id=1, source_target_pairs={{0,1},{1,0},{2,3},{3,2},{4,5},{5,4},{6,7},{7,6},{32,34},{33,35},{3... | collective-permute-start | bytes 147464 | tf_op jit(solution)/shard_map/ppermute | solution.py:452
  67.6 5.1 %collective-permute-start.20 = (bf16[96,256]{1,0:T(8,128)(2,1)S(1)}, bf16[96,256]{1,0:T(8,128)(2,1)S(1)}, u32[]{:S(2)}, u32[]{:S(2)}) collective-permute-start(bf16[96,256]{1,0:T(8,128)(2,1)S(1)} %add_convert_fusion.4), channel_id=1, source_target_pairs={{0,40},{8,32},{32,72},{40,64},{64,104},{72,96},{96,8},{104,0},{1,4... | collective-permute-start | bytes 147464 | tf_op jit(solution)/shard_map/ppermute | solution.py:459
  70.6 4.2 %collective-permute-start.18 = (bf16[96,256]{1,0:T(8,128)(2,1)S(1)}, bf16[96,256]{1,0:T(8,128)(2,1)S(1)}, u32[]{:S(2)}, u32[]{:S(2)}) collective-permute-start(bf16[96,256]{1,0:T(8,128)(2,1)S(1)} %add_convert_fusion.4), channel_id=1, source_target_pairs={{0,32},{32,64},{64,96},{96,0},{1,33},{33,65},{65,97},{97,1},{2,34}... | collective-permute-start | bytes 147464 | tf_op jit(solution)/shard_map/ppermute | solution.py:458
  72.7 5.2 %collective-permute-start.21 = (bf16[96,256]{1,0:T(8,128)(2,1)S(1)}, bf16[96,256]{1,0:T(8,128)(2,1)S(1)}, u32[]{:S(2)}, u32[]{:S(2)}) collective-permute-start(bf16[96,256]{1,0:T(8,128)(2,1)S(1)} %collective-permute-done.20.c_ref), channel_id=1, source_target_pairs={{0,1},{1,0},{2,3},{3,2},{4,5},{5,4},{6,7},{7,6},{8,9},{9,8},{10,11... | collective-permute-start | bytes 147464 | tf_op jit(solution)/shard_map/ppermute | solution.py:359
  74.7 4.1 %collective-permute-start.19 = (bf16[96,256]{1,0:T(8,128)(2,1)S(1)}, bf16[96,256]{1,0:T(8,128)(2,1)S(1)}, u32[]{:S(2)}, u32[]{:S(2)}) collective-permute-start(bf16[96,256]{1,0:T(8,128)(2,1)S(1)} %collective-permute-done.18.a_ref), channel_id=1, source_target_pairs={{0,1},{1,0},{2,3},{3,2},{4,5},{5,4},{6,7},{7,6},{8,9},{9,8},{10,11... | collective-permute-start | bytes 147464 | tf_op jit(solution)/shard_map/ppermute | solution.py:359
  80.2 1.3 %collective-permute-start.22 = (bf16[96,256]{1,0:T(8,128)(2,1)S(1)}, bf16[96,256]{1,0:T(8,128)(2,1)S(1)}, u32[]{:S(2)}, u32[]{:S(2)}) collective-permute-start(bf16[96,256]{1,0:T(8,128)(2,1)S(1)} %get-tuple-element.34), channel_id=1, source_target_pairs={{0,1},{1,0},{2,3},{3,2},{4,5},{5,4},{6,7},{7,6},{8,9},{9,8},{10,11... | collective-permute-start | bytes 147464 | tf_op jit(solution)/shard_map/ppermute | solution.py:359
  81.5 1.3 %collective-permute-start.25 = (bf16[96,256]{1,0:T(8,128)(2,1)S(1)}, bf16[96,256]{1,0:T(8,128)(2,1)S(1)}, u32[]{:S(2)}, u32[]{:S(2)}) collective-permute-start(bf16[96,256]{1,0:T(8,128)(2,1)S(1)} %add_convert_fusion.3), channel_id=1, source_target_pairs={{0,1},{1,0},{2,3},{3,2},{4,5},{5,4},{6,7},{7,6},{32,33},{33,32},{3... | collective-permute-start | bytes 147464 | tf_op jit(solution)/shard_map/ppermute | solution.py:452
  82.0 1.2 %collective-permute-start.24 = (bf16[96,256]{1,0:T(8,128)(2,1)S(1)}, bf16[96,256]{1,0:T(8,128)(2,1)S(1)}, u32[]{:S(2)}, u32[]{:S(2)}) collective-permute-start(bf16[96,256]{1,0:T(8,128)(2,1)S(1)} %add_convert_fusion.3), channel_id=1, source_target_pairs={{0,1},{1,0},{2,3},{3,2},{4,5},{5,4},{6,7},{7,6},{32,33},{33,32},{3... | collective-permute-start | bytes 147464 | tf_op jit(solution)/shard_map/ppermute | solution.py:452
  82.1 1.2 %collective-permute-start.23 = (bf16[96,256]{1,0:T(8,128)(2,1)S(1)}, bf16[96,256]{1,0:T(8,128)(2,1)S(1)}, u32[]{:S(2)}, u32[]{:S(2)}) collective-permute-start(bf16[96,256]{1,0:T(8,128)(2,1)S(1)} %add_convert_fusion.3), channel_id=1, source_target_pairs={{0,1},{1,0},{2,3},{3,2},{4,5},{5,4},{6,7},{7,6},{32,33},{33,32},{3... | collective-permute-start | bytes 147464 | tf_op jit(solution)/shard_map/ppermute | solution.py:452
  83.4 5.3 %collective-permute-start.28 = (bf16[96,256]{1,0:T(8,128)(2,1)S(1)}, bf16[96,256]{1,0:T(8,128)(2,1)S(1)}, u32[]{:S(2)}, u32[]{:S(2)}) collective-permute-start(bf16[96,256]{1,0:T(8,128)(2,1)S(1)} %add_convert_fusion.1), channel_id=1, source_target_pairs={{0,40},{8,32},{32,72},{40,64},{64,104},{72,96},{96,8},{104,0},{1,4... | collective-permute-start | bytes 147464 | tf_op jit(solution)/shard_map/ppermute | solution.py:459
  83.7 6.8 %collective-permute-start.26 = (bf16[96,256]{1,0:T(8,128)(2,1)S(1)}, bf16[96,256]{1,0:T(8,128)(2,1)S(1)}, u32[]{:S(2)}, u32[]{:S(2)}) collective-permute-start(bf16[96,256]{1,0:T(8,128)(2,1)S(1)} %add_convert_fusion.1), channel_id=1, source_target_pairs={{0,32},{32,64},{64,96},{96,0},{1,33},{33,65},{65,97},{97,1},{2,34}... | collective-permute-start | bytes 147464 | tf_op jit(solution)/shard_map/ppermute | solution.py:458
  88.7 2.6 %collective-permute-start.29 = (bf16[96,256]{1,0:T(8,128)(2,1)S(1)}, bf16[96,256]{1,0:T(8,128)(2,1)S(1)}, u32[]{:S(2)}, u32[]{:S(2)}) collective-permute-start(bf16[96,256]{1,0:T(8,128)(2,1)S(1)} %collective-permute-done.28.c_ref), channel_id=1, source_target_pairs={{0,1},{1,0},{2,3},{3,2},{4,5},{5,4},{6,7},{7,6},{8,9},{9,8},{10,11... | collective-permute-start | bytes 147464 | tf_op jit(solution)/shard_map/ppermute | solution.py:359
  90.4 1.2 %collective-permute-start.27 = (bf16[96,256]{1,0:T(8,128)(2,1)S(1)}, bf16[96,256]{1,0:T(8,128)(2,1)S(1)}, u32[]{:S(2)}, u32[]{:S(2)}) collective-permute-start(bf16[96,256]{1,0:T(8,128)(2,1)S(1)} %collective-permute-done.26.a_ref.mine_ref), channel_id=1, source_target_pairs={{0,1},{1,0},{2,3},{3,2},{4,5},{5,4},{6,7},{7,6},{8,9},{9,8},{10,11... | collective-permute-start | bytes 147464 | tf_op jit(solution)/shard_map/ppermute | solution.py:359
  93.1 1.3 %collective-permute-start.30 = (bf16[96,256]{1,0:T(8,128)(2,1)S(1)}, bf16[96,256]{1,0:T(8,128)(2,1)S(1)}, u32[]{:S(2)}, u32[]{:S(2)}) collective-permute-start(bf16[96,256]{1,0:T(8,128)(2,1)S(1)} %get-tuple-element.36), channel_id=1, source_target_pairs={{0,1},{1,0},{2,3},{3,2},{4,5},{5,4},{6,7},{7,6},{8,9},{9,8},{10,11... | collective-permute-start | bytes 147464 | tf_op jit(solution)/shard_map/ppermute | solution.py:359
  94.4 1.3 %collective-permute-start.33 = (bf16[96,256]{1,0:T(8,128)(2,1)S(1)}, bf16[96,256]{1,0:T(8,128)(2,1)S(1)}, u32[]{:S(2)}, u32[]{:S(2)}) collective-permute-start(bf16[96,256]{1,0:T(8,128)(2,1)S(1)} %add_convert_fusion.m0_ref), channel_id=1, source_target_pairs={{0,1},{1,0},{2,3},{3,2},{4,5},{5,4},{6,7},{7,6},{32,33},{33,32},{3... | collective-permute-start | bytes 147464 | tf_op jit(solution)/shard_map/ppermute | solution.py:452
  94.8 1.2 %collective-permute-start.32 = (bf16[96,256]{1,0:T(8,128)(2,1)S(1)}, bf16[96,256]{1,0:T(8,128)(2,1)S(1)}, u32[]{:S(2)}, u32[]{:S(2)}) collective-permute-start(bf16[96,256]{1,0:T(8,128)(2,1)S(1)} %add_convert_fusion.m0_ref), channel_id=1, source_target_pairs={{0,1},{1,0},{2,3},{3,2},{4,5},{5,4},{6,7},{7,6},{32,33},{33,32},{3... | collective-permute-start | bytes 147464 | tf_op jit(solution)/shard_map/ppermute | solution.py:452
  95.0 1.2 %collective-permute-start.31 = (bf16[96,256]{1,0:T(8,128)(2,1)S(1)}, bf16[96,256]{1,0:T(8,128)(2,1)S(1)}, u32[]{:S(2)}, u32[]{:S(2)}) collective-permute-start(bf16[96,256]{1,0:T(8,128)(2,1)S(1)} %add_convert_fusion.m0_ref), channel_id=1, source_target_pairs={{0,1},{1,0},{2,3},{3,2},{4,5},{5,4},{6,7},{7,6},{32,33},{33,32},{3... | collective-permute-start | bytes 147464 | tf_op jit(solution)/shard_map/ppermute | solution.py:452
where the time goes:
time: 114 us; the launch traced here: 113 us
  waiting for transfers between devices  37.5 us (33%)
  blocking collectives  35.1 us (31%)
  starting transfers between devices  31.2 us (27%)
  Pallas kernels  8.48 us (7%)
    ppermute x16, waiting for transfers between devices, flip(): return lax.ppermute(v, axes, [(i, i ^ bits) for i in range(size)])  22.9 us
    all_to_all x1, blocking collectives, per_device(): recv = lax.all_to_all(send, BLOCKS, 0, 0)  19 us
    ppermute x16, starting transfers between devices, flip(): return lax.ppermute(v, axes, [(i, i ^ bits) for i in range(size)])  18.9 us
    all_to_all x1, blocking collectives, per_device(): recv = lax.all_to_all(send, ('pp', 'ym', 'yh', 'tc'), 0, 0)  16.1 us
    ppermute x3, waiting for transfers between devices, per_device(): c = lax.ppermute(produced, ('pp', 'yh'), hop_flip)  9.14 us
    ppermute x12, starting transfers between devices, per_device(): lax.ppermute(mixed, ('pp', 'tz', 'tc'), sum_pairs(s, sections, d))  5.87 us
    ppermute x12, waiting for transfers between devices, per_device(): lax.ppermute(mixed, ('pp', 'tz', 'tc'), sum_pairs(s, sections, d))  5.1 us
    pallas_call x3, Pallas kernels, per_device(): call_kernel(relay_section_kernel, outs, 13, [pad])  4.26 us
  transfers between devices with their start and end apart: 34, of which 26 were waited for; matrix products, arithmetic and copies ran while one was open for 0% of the time, Pallas kernels for 0%

commit v1 on v0

--- a/solution.py
+++ b/solution.py
@@ -229,7 +229,7 @@
     diagonal = row_id == col_id
     pairs = []
     for i in range(2):
-        high = []
+        high, rest = [], []
         for j in (2 * i, 2 * i + 1):
             fc = cum_cols[:, 2 * j : 2 * j + 1]
             bc = cum_cols[:, 2 * j + 1 : 2 * j + 2]
@@ -241,7 +241,9 @@
             mix = mix + jnp.where(diagonal, d1, 0.0)
             combined = scores * mix
             high.append(combined.astype(BF16))
-        y = nn_dot(jnp.concatenate(high, axis=0), acts[i])
+            rest.append((combined - high[-1].astype(F32)).astype(BF16))
+        y = nn_dot(jnp.concatenate(high + rest, axis=0), acts[i])
+        y = y[: 2 * T] + y[2 * T :]
         skip = jnp.where(low_row, *[small[2 * i + e][1][:, 256:384] for e in range(2)])
         y = jnp.where(low, y[:T], y[T:]) + skip * acts[i].astype(F32)
         gate = pad_ref[8 : 8 + T, 512 + 128 * i : 640 + 128 * i]

time: 114 us -> 114 us (level)
  no operation moved by 1% of the time
where the time goes in v1:
time: 114 us; the launch traced here: 113 us
  waiting for transfers between devices  37.5 us (33%)
  blocking collectives  35.1 us (31%)
  starting transfers between devices  31.2 us (27%)
  Pallas kernels  8.53 us (7%)
    ppermute x16, waiting for transfers between devices, flip(): return lax.ppermute(v, axes, [(i, i ^ bits) for i in range(size)])  22.9 us
    all_to_all x1, blocking collectives, per_device(): recv = lax.all_to_all(send, BLOCKS, 0, 0)  19 us
    ppermute x16, starting transfers between devices, flip(): return lax.ppermute(v, axes, [(i, i ^ bits) for i in range(size)])  18.9 us
    all_to_all x1, blocking collectives, per_device(): recv = lax.all_to_all(send, ('pp', 'ym', 'yh', 'tc'), 0, 0)  16.1 us
    ppermute x3, waiting for transfers between devices, per_device(): c = lax.ppermute(produced, ('pp', 'yh'), hop_flip)  9.14 us
    ppermute x12, starting transfers between devices, per_device(): lax.ppermute(mixed, ('pp', 'tz', 'tc'), sum_pairs(s, sections, d))  5.88 us
    ppermute x12, waiting for transfers between devices, per_device(): lax.ppermute(mixed, ('pp', 'tz', 'tc'), sum_pairs(s, sections, d))  5.09 us
    pallas_call x3, Pallas kernels, per_device(): call_kernel(relay_section_kernel, outs, 13, [pad])  4.29 us
  transfers between devices with their start and end apart: 34, of which 26 were waited for; matrix products, arithmetic and copies ran while one was open for 0% of the time, Pallas kernels for 0%

profile of v1, /device:TPU:1, one launch (start us, length us, event | category | flops | bytes accessed | tf_op | source)
XLA Modules:
  0.0 113.4 jit_solution(10201040331786447919)
XLA Ops:
  0.8 1.5 %shard_map.136 = (bf16[24,32]{1,0:T(8,128)(2,1)S(1)}, bf16[24,32]{1,0:T(8,128)(2,1)S(1)}, bf16[168,1024]{1,0:T(8,128)(2,1)S(1)}, bf16[168,1024]{1,0:T(8,128)(2,1...) custom-call(s32[5,256]{1,0:T(8,128)S(1)} %broadcast_in_dim.2.where_ref, ...), custom_call_target="tpu_custom_call" | custom-call | tf_op jit(solution)/shard_map/pallas_call | solution.py:414
  2.4 3.6 %collective-permute-start.5 = (bf16[168,1024]{1,0:T(8,128)(2,1)S(1)}, bf16[168,1024]{1,0:T(8,128)(2,1)S(1)}, u32[]{:S(2)}, u32[]{:S(2)}) collective-permute-start(bf16[168,1024]{1,0:T(8,128)(2,1)S(1)} %get-tuple-element.24), channel_id=1, source_target_pairs={{0,24},{8,16},{16,8},{24,0},{1,25},{9,17},{17,9},{25,1},{2,26},{10... | collective-permute-start | bytes 1032200 | tf_op jit(solution)/shard_map/ppermute | solution.py:361
  6.0 1.3 %collective-permute-start.4 = (bf16[168,1024]{1,0:T(8,128)(2,1)S(1)}, bf16[168,1024]{1,0:T(8,128)(2,1)S(1)}, u32[]{:S(2)}, u32[]{:S(2)}) collective-permute-start(bf16[168,1024]{1,0:T(8,128)(2,1)S(1)} %get-tuple-element.23.refs_0_), channel_id=1, source_target_pairs={{0,16},{8,24},{16,0},{24,8},{1,17},{9,25},{17,1},{25,9},{2,18},{10... | collective-permute-start | bytes 1032200 | tf_op jit(solution)/shard_map/ppermute | solution.py:361
  7.3 0.2 collective-permute-start
  7.5 2.4 %collective-permute-start.2 = (bf16[24,32]{1,0:T(8,128)(2,1)S(1)}, bf16[24,32]{1,0:T(8,128)(2,1)S(1)}, u32[]{:S(2)}, u32[]{:S(2)}) collective-permute-start(bf16[24,32]{1,0:T(8,128)(2,1)S(1)} %get-tuple-element.22), channel_id=1, source_target_pairs={{0,24},{8,16},{16,8},{24,0},{1,25},{9,17},{17,9},{25,1},{2,26},{10... | collective-permute-start | bytes 4616 | tf_op jit(solution)/shard_map/ppermute | solution.py:361
  9.9 12.3 %collective-permute-done.r1_ref = bf16[24,32]{1,0:T(8,128)(2,1)S(1)} collective-permute-done((bf16[24,32]{1,0:T(8,128)(2,1)S(1)}, bf16[24,32]{1,0:T(8,128)(2,1)S(1)}, u32[]{:S(2)}, u32[]{:S(2)}) %collective-permute-start) | collective-permute-done | bytes 1568 | tf_op jit(solution)/shard_map/ppermute | solution.py:361
  22.2 0.3 collective-permute-start.1
  22.5 3.6 %collective-permute-done.1.r2_ref = bf16[24,32]{1,0:T(8,128)(2,1)S(1)} collective-permute-done((bf16[24,32]{1,0:T(8,128)(2,1)S(1)}, bf16[24,32]{1,0:T(8,128)(2,1)S(1)}, u32[]{:S(2)}, u32[]{:S(2)}) %collective-permute-start.1) | collective-permute-done | bytes 1568 | tf_op jit(solution)/shard_map/ppermute | solution.py:361
  26.3 19.0 %all_to_all.10.recv_ref = bf16[32,24,128]{2,1,0:T(8,128)(2,1)S(1)} all-to-all(bf16[32,24,128]{2,1,0:T(8,128)(2,1)S(1)} %shard_map.137), channel_id=1, replica_groups=mesh['pp'=4,'ym'=2,'yh'=2,'tz'=4,'tc'=2] {'pp','tz','tc'}, dimensions={0} | all-to-all | bytes 393216 | tf_op jit(solution)/shard_map/all_to_all | solution.py:438
  45.3 1.6 %shard_map.138 = (bf16[96,256]{1,0:T(8,128)(2,1)S(1)}, f32[96,256]{1,0:T(8,128)S(1)}, bf16[96,256]{1,0:T(8,128)(2,1)S(1)}) custom-call(s32[5,256]{1,0:T(8,128)S(1)} %broadcast_in_dim.2.where_ref, bf16[32,24,128]{2,1,0:T(8,128)(2,1)S(1)} %all_to_all.10.recv_ref, bf16[168,1024]{1,0:T(8,128)(2,1)S(1)} %get-tuple-element.23.refs_0_, ...), custom_call_target="tpu_custom_call" | custom-call | tf_op jit(solution)/shard_map/pallas_call | solution.py:444
  46.9 0.4 collective-permute-start.6
  47.2 0.9 collective-permute-done.6
  48.2 1.0 collective-permute-start.9
  49.2 1.1 collective-permute-start.8
  50.3 1.2 %collective-permute-start.7 = (bf16[96,256]{1,0:T(8,128)(2,1)S(1)}, bf16[96,256]{1,0:T(8,128)(2,1)S(1)}, u32[]{:S(2)}, u32[]{:S(2)}) collective-permute-start(bf16[96,256]{1,0:T(8,128)(2,1)S(1)} %add_convert_fusion.9), channel_id=1, source_target_pairs={{0,2},{1,3},{2,0},{3,1},{4,6},{5,7},{6,4},{7,5},{32,33},{33,32},{3... | collective-permute-start | bytes 147464 | tf_op jit(solution)/shard_map/ppermute | solution.py:454
  51.5 0.9 collective-permute-done.9
  52.4 1.3 %collective-permute-done.8 = bf16[96,256]{1,0:T(8,128)(2,1)S(1)} collective-permute-done((bf16[96,256]{1,0:T(8,128)(2,1)S(1)}, bf16[96,256]{1,0:T(8,128)(2,1)S(1)}, u32[]{:S(2)}, u32[]{:S(2)}) %collective-permute-start.8) | collective-permute-done | bytes 49184 | tf_op jit(solution)/shard_map/ppermute | solution.py:454
  53.9 5.0 %collective-permute-done.12.c_ref = bf16[96,256]{1,0:T(8,128)(2,1)S(1)} collective-permute-done((bf16[96,256]{1,0:T(8,128)(2,1)S(1)}, bf16[96,256]{1,0:T(8,128)(2,1)S(1)}, u32[]{:S(2)}, u32[]{:S(2)}) %collective-permute-start.12) | collective-permute-done | bytes 49184 | tf_op jit(solution)/shard_map/ppermute | solution.py:461
  58.9 2.8 %collective-permute-start.13 = (bf16[96,256]{1,0:T(8,128)(2,1)S(1)}, bf16[96,256]{1,0:T(8,128)(2,1)S(1)}, u32[]{:S(2)}, u32[]{:S(2)}) collective-permute-start(bf16[96,256]{1,0:T(8,128)(2,1)S(1)} %collective-permute-done.12.c_ref), channel_id=1, source_target_pairs={{0,1},{1,0},{2,3},{3,2},{4,5},{5,4},{6,7},{7,6},{8,9},{9,8},{10,11... | collective-permute-start | bytes 147464 | tf_op jit(solution)/shard_map/ppermute | solution.py:361
  61.7 0.9 collective-permute-done.13.d_ref
  62.6 0.4 collective-permute-done.11.b_ref
  62.9 1.4 %shard_map.139 = (f32[96,256]{1,0:T(8,128)S(1)}, bf16[96,256]{1,0:T(8,128)(2,1)S(1)}) custom-call(s32[5,256]{1,0:T(8,128)S(1)} %broadcast_in_dim.2.where_ref, bf16[96,256]{1,0:T(8,128)(2,1)S(1)} %collective-permute-done.10.a_ref, bf16[96,256]{1,0:T(8,128)(2,1)S(1)} %collective-permute-done.11.b_ref, bf16[96,256]{1,0:T(8,128)(2,1)S(1)} %collective-permute-done.12.c_ref, ...), custom_call_target="tpu_custom_call" | custom-call | tf_op jit(solution)/shard_map/pallas_call | solution.py:465
  64.4 0.2 collective-permute-start.14
  64.6 1.1 collective-permute-done.14
  65.7 0.2 collective-permute-start.17
  65.9 0.3 collective-permute-start.16
  66.3 0.2 collective-permute-start.15
  66.5 0.6 collective-permute-done.17
  67.0 0.2 collective-permute-done.16
  67.2 0.3 collective-permute-done.15
  67.6 3.0 %collective-permute-start.20 = (bf16[96,256]{1,0:T(8,128)(2,1)S(1)}, bf16[96,256]{1,0:T(8,128)(2,1)S(1)}, u32[]{:S(2)}, u32[]{:S(2)}) collective-permute-start(bf16[96,256]{1,0:T(8,128)(2,1)S(1)} %add_convert_fusion.4), channel_id=1, source_target_pairs={{0,40},{8,32},{32,72},{40,64},{64,104},{72,96},{96,8},{104,0},{1,4... | collective-permute-start | bytes 147464 | tf_op jit(solution)/shard_map/ppermute | solution.py:461
  70.6 2.1 %collective-permute-done.20.c_ref = bf16[96,256]{1,0:T(8,128)(2,1)S(1)} collective-permute-done((bf16[96,256]{1,0:T(8,128)(2,1)S(1)}, bf16[96,256]{1,0:T(8,128)(2,1)S(1)}, u32[]{:S(2)}, u32[]{:S(2)}) %collective-permute-start.20) | collective-permute-done | bytes 49184 | tf_op jit(solution)/shard_map/ppermute | solution.py:461
  72.7 1.7 %collective-permute-start.21 = (bf16[96,256]{1,0:T(8,128)(2,1)S(1)}, bf16[96,256]{1,0:T(8,128)(2,1)S(1)}, u32[]{:S(2)}, u32[]{:S(2)}) collective-permute-start(bf16[96,256]{1,0:T(8,128)(2,1)S(1)} %collective-permute-done.20.c_ref), channel_id=1, source_target_pairs={{0,1},{1,0},{2,3},{3,2},{4,5},{5,4},{6,7},{7,6},{8,9},{9,8},{10,11... | collective-permute-start | bytes 147464 | tf_op jit(solution)/shard_map/ppermute | solution.py:361
  74.4 0.4 collective-permute-done.18.a_ref
  74.7 3.2 %collective-permute-start.19 = (bf16[96,256]{1,0:T(8,128)(2,1)S(1)}, bf16[96,256]{1,0:T(8,128)(2,1)S(1)}, u32[]{:S(2)}, u32[]{:S(2)}) collective-permute-start(bf16[96,256]{1,0:T(8,128)(2,1)S(1)} %collective-permute-done.18.a_ref), channel_id=1, source_target_pairs={{0,1},{1,0},{2,3},{3,2},{4,5},{5,4},{6,7},{7,6},{8,9},{9,8},{10,11... | collective-permute-start | bytes 147464 | tf_op jit(solution)/shard_map/ppermute | solution.py:361
  77.9 0.9 collective-permute-done.19.b_ref
  78.8 1.4 %shard_map.140 = (f32[96,256]{1,0:T(8,128)S(1)}, bf16[96,256]{1,0:T(8,128)(2,1)S(1)}) custom-call(s32[5,256]{1,0:T(8,128)S(1)} %broadcast_in_dim.2.where_ref, bf16[96,256]{1,0:T(8,128)(2,1)S(1)} %collective-permute-done.18.a_ref, bf16[96,256]{1,0:T(8,128)(2,1)S(1)} %collective-permute-done.19.b_ref, bf16[96,256]{1,0:T(8,128)(2,1)S(1)} %collective-permute-done.20.c_ref, ...), custom_call_target="tpu_custom_call" | custom-call | tf_op jit(solution)/shard_map/pallas_call | solution.py:465
  80.2 0.4 collective-permute-start.22
  80.7 0.9 collective-permute-done.22
  81.6 0.4 collective-permute-start.25
  82.0 0.2 collective-permute-start.24
  82.1 0.3 collective-permute-start.23
  82.5 0.4 collective-permute-done.25
  82.9 0.3 collective-permute-done.24
  83.2 0.2 collective-permute-done.23
  83.4 0.3 collective-permute-start.28
  83.7 2.9 %collective-permute-start.26 = (bf16[96,256]{1,0:T(8,128)(2,1)S(1)}, bf16[96,256]{1,0:T(8,128)(2,1)S(1)}, u32[]{:S(2)}, u32[]{:S(2)}) collective-permute-start(bf16[96,256]{1,0:T(8,128)(2,1)S(1)} %add_convert_fusion.1), channel_id=1, source_target_pairs={{0,32},{32,64},{64,96},{96,0},{1,33},{33,65},{65,97},{97,1},{2,34}... | collective-permute-start | bytes 147464 | tf_op jit(solution)/shard_map/ppermute | solution.py:460
  86.6 2.1 %collective-permute-done.28.c_ref = bf16[96,256]{1,0:T(8,128)(2,1)S(1)} collective-permute-done((bf16[96,256]{1,0:T(8,128)(2,1)S(1)}, bf16[96,256]{1,0:T(8,128)(2,1)S(1)}, u32[]{:S(2)}, u32[]{:S(2)}) %collective-permute-start.28) | collective-permute-done | bytes 49184 | tf_op jit(solution)/shard_map/ppermute | solution.py:461
  88.7 1.7 %collective-permute-start.29 = (bf16[96,256]{1,0:T(8,128)(2,1)S(1)}, bf16[96,256]{1,0:T(8,128)(2,1)S(1)}, u32[]{:S(2)}, u32[]{:S(2)}) collective-permute-start(bf16[96,256]{1,0:T(8,128)(2,1)S(1)} %collective-permute-done.28.c_ref), channel_id=1, source_target_pairs={{0,1},{1,0},{2,3},{3,2},{4,5},{5,4},{6,7},{7,6},{8,9},{9,8},{10,11... | collective-permute-start | bytes 147464 | tf_op jit(solution)/shard_map/ppermute | solution.py:361
  90.5 0.3 collective-permute-start.27
  90.7 0.6 collective-permute-done.29.d_ref
  91.3 0.4 collective-permute-done.27.b_ref
  91.7 1.4 %shard_map.141 = (f32[96,256]{1,0:T(8,128)S(1)}, bf16[96,256]{1,0:T(8,128)(2,1)S(1)}) custom-call(s32[5,256]{1,0:T(8,128)S(1)} %broadcast_in_dim.2.where_ref, bf16[96,256]{1,0:T(8,128)(2,1)S(1)} %collective-permute-done.26.a_ref.mine_ref, bf16[96,256]{1,0:T(8,128)(2,1)S(1)} %collective-permute-done.27.b_ref, ...), custom_call_target="tpu_custom_call" | custom-call | tf_op jit(solution)/shard_map/pallas_call | solution.py:465
  93.1 0.3 collective-permute-start.30
  93.5 1.0 collective-permute-done.30
  94.5 0.3 collective-permute-start.33
  94.8 0.2 collective-permute-start.32
  95.0 0.3 collective-permute-start.31
  95.3 0.5 collective-permute-done.33.m3_ref
  95.8 0.3 collective-permute-done.32.m2_ref
  96.0 0.2 collective-permute-done.31.m1_ref
  96.3 0.2 shard_map.142
  96.5 16.1 %all_to_all.11.recv_ref = bf16[32,8,128]{2,1,0:T(8,128)(2,1)S(1)} all-to-all(bf16[32,8,128]{2,1,0:T(8,128)(2,1)S(1)} %shard_map.142), channel_id=1, replica_groups=mesh['pp'=4,'ym'=2,'yh'=2,'tz'=4,'tc'=2] {'pp','ym','yh','tc'}, dimensions={0} | all-to-all | bytes 131072 | tf_op jit(solution)/shard_map/all_to_all | solution.py:468
  112.6 0.8 shard_map.143
  (27 shorter events, 0.6 us)
Async XLA Ops:
  2.4 42.9 %collective-permute-start.5 = (bf16[168,1024]{1,0:T(8,128)(2,1)S(1)}, bf16[168,1024]{1,0:T(8,128)(2,1)S(1)}, u32[]{:S(2)}, u32[]{:S(2)}) collective-permute-start(bf16[168,1024]{1,0:T(8,128)(2,1)S(1)} %get-tuple-element.24), channel_id=1, source_target_pairs={{0,24},{8,16},{16,8},{24,0},{1,25},{9,17},{17,9},{25,1},{2,26},{10... | collective-permute-start | bytes 1032200 | tf_op jit(solution)/shard_map/ppermute | solution.py:361
  6.0 39.3 %collective-permute-start.3 = (bf16[168,1024]{1,0:T(8,128)(2,1)S(1)}, bf16[168,1024]{1,0:T(8,128)(2,1)S(1)}, u32[]{:S(2)}, u32[]{:S(2)}) collective-permute-start(bf16[168,1024]{1,0:T(8,128)(2,1)S(1)} %get-tuple-element.24), channel_id=1, source_target_pairs={{0,8},{8,0},{16,24},{24,16},{1,9},{9,1},{17,25},{25,17},{2,10},{10... | collective-permute-start | bytes 1032200 | tf_op jit(solution)/shard_map/ppermute | solution.py:361
  6.0 39.3 %collective-permute-start.4 = (bf16[168,1024]{1,0:T(8,128)(2,1)S(1)}, bf16[168,1024]{1,0:T(8,128)(2,1)S(1)}, u32[]{:S(2)}, u32[]{:S(2)}) collective-permute-start(bf16[168,1024]{1,0:T(8,128)(2,1)S(1)} %get-tuple-element.23.refs_0_), channel_id=1, source_target_pairs={{0,16},{8,24},{16,0},{24,8},{1,17},{9,25},{17,1},{25,9},{2,18},{10... | collective-permute-start | bytes 1032200 | tf_op jit(solution)/shard_map/ppermute | solution.py:361
  7.3 14.9 %collective-permute-start = (bf16[24,32]{1,0:T(8,128)(2,1)S(1)}, bf16[24,32]{1,0:T(8,128)(2,1)S(1)}, u32[]{:S(2)}, u32[]{:S(2)}) collective-permute-start(bf16[24,32]{1,0:T(8,128)(2,1)S(1)} %get-tuple-element.21.r0_ref), channel_id=1, source_target_pairs={{0,8},{8,0},{16,24},{24,16},{1,9},{9,1},{17,25},{25,17},{2,10},{10... | collective-permute-start | bytes 4616 | tf_op jit(solution)/shard_map/ppermute | solution.py:361
  7.5 37.8 %copy-start = (bf16[1,1024,1,128]{3,1,2,0:T(8,128)(2,1)S(1)}, bf16[1,1024,1,128]{3,1,2,0:T(8,128)(2,1)}, u32[]{:S(2)}) copy-start(bf16[1,1024,1,128]{3,1,2,0:T(8,128)(2,1)} %param.18) | copy-start | bytes 786436
  7.5 37.8 %copy-start.1 = (bf16[1,1024,1,128]{3,1,2,0:T(8,128)(2,1)S(1)}, bf16[1,1024,1,128]{3,1,2,0:T(8,128)(2,1)}, u32[]{:S(2)}) copy-start(bf16[1,1024,1,128]{3,1,2,0:T(8,128)(2,1)} %param.19) | copy-start | bytes 786436
  7.5 15.1 %collective-permute-start.2 = (bf16[24,32]{1,0:T(8,128)(2,1)S(1)}, bf16[24,32]{1,0:T(8,128)(2,1)S(1)}, u32[]{:S(2)}, u32[]{:S(2)}) collective-permute-start(bf16[24,32]{1,0:T(8,128)(2,1)S(1)} %get-tuple-element.22), channel_id=1, source_target_pairs={{0,24},{8,16},{16,8},{24,0},{1,25},{9,17},{17,9},{25,1},{2,26},{10... | collective-permute-start | bytes 4616 | tf_op jit(solution)/shard_map/ppermute | solution.py:361
  22.2 4.0 %collective-permute-start.1 = (bf16[24,32]{1,0:T(8,128)(2,1)S(1)}, bf16[24,32]{1,0:T(8,128)(2,1)S(1)}, u32[]{:S(2)}, u32[]{:S(2)}) collective-permute-start(bf16[24,32]{1,0:T(8,128)(2,1)S(1)} %get-tuple-element.22), channel_id=1, source_target_pairs={{0,16},{8,24},{16,0},{24,8},{1,17},{9,25},{17,1},{25,9},{2,18},{10... | collective-permute-start | bytes 4616 | tf_op jit(solution)/shard_map/ppermute | solution.py:361
  46.9 1.3 %collective-permute-start.6 = (bf16[96,256]{1,0:T(8,128)(2,1)S(1)}, bf16[96,256]{1,0:T(8,128)(2,1)S(1)}, u32[]{:S(2)}, u32[]{:S(2)}) collective-permute-start(bf16[96,256]{1,0:T(8,128)(2,1)S(1)} %get-tuple-element.30), channel_id=1, source_target_pairs={{0,1},{1,0},{2,3},{3,2},{4,5},{5,4},{6,7},{7,6},{8,9},{9,8},{10,11... | collective-permute-start | bytes 147464 | tf_op jit(solution)/shard_map/ppermute | solution.py:361
  48.2 4.2 %collective-permute-start.9 = (bf16[96,256]{1,0:T(8,128)(2,1)S(1)}, bf16[96,256]{1,0:T(8,128)(2,1)S(1)}, u32[]{:S(2)}, u32[]{:S(2)}) collective-permute-start(bf16[96,256]{1,0:T(8,128)(2,1)S(1)} %add_convert_fusion.9), channel_id=1, source_target_pairs={{0,6},{1,7},{2,4},{3,5},{4,2},{5,3},{6,0},{7,1},{32,33},{33,32},{3... | collective-permute-start | bytes 147464 | tf_op jit(solution)/shard_map/ppermute | solution.py:454
  49.2 4.5 %collective-permute-start.8 = (bf16[96,256]{1,0:T(8,128)(2,1)S(1)}, bf16[96,256]{1,0:T(8,128)(2,1)S(1)}, u32[]{:S(2)}, u32[]{:S(2)}) collective-permute-start(bf16[96,256]{1,0:T(8,128)(2,1)S(1)} %add_convert_fusion.9), channel_id=1, source_target_pairs={{0,4},{1,5},{2,6},{3,7},{4,0},{5,1},{6,2},{7,3},{32,33},{33,32},{3... | collective-permute-start | bytes 147464 | tf_op jit(solution)/shard_map/ppermute | solution.py:454
  50.3 3.4 %collective-permute-start.7 = (bf16[96,256]{1,0:T(8,128)(2,1)S(1)}, bf16[96,256]{1,0:T(8,128)(2,1)S(1)}, u32[]{:S(2)}, u32[]{:S(2)}) collective-permute-start(bf16[96,256]{1,0:T(8,128)(2,1)S(1)} %add_convert_fusion.9), channel_id=1, source_target_pairs={{0,2},{1,3},{2,0},{3,1},{4,6},{5,7},{6,4},{7,5},{32,33},{33,32},{3... | collective-permute-start | bytes 147464 | tf_op jit(solution)/shard_map/ppermute | solution.py:454
  53.7 5.1 %collective-permute-start.12 = (bf16[96,256]{1,0:T(8,128)(2,1)S(1)}, bf16[96,256]{1,0:T(8,128)(2,1)S(1)}, u32[]{:S(2)}, u32[]{:S(2)}) collective-permute-start(bf16[96,256]{1,0:T(8,128)(2,1)S(1)} %add_convert_fusion.7), channel_id=1, source_target_pairs={{0,40},{8,32},{32,72},{40,64},{64,104},{72,96},{96,8},{104,0},{1,4... | collective-permute-start | bytes 147464 | tf_op jit(solution)/shard_map/ppermute | solution.py:461
  53.8 7.9 %collective-permute-start.10 = (bf16[96,256]{1,0:T(8,128)(2,1)S(1)}, bf16[96,256]{1,0:T(8,128)(2,1)S(1)}, u32[]{:S(2)}, u32[]{:S(2)}) collective-permute-start(bf16[96,256]{1,0:T(8,128)(2,1)S(1)} %add_convert_fusion.7), channel_id=1, source_target_pairs={{0,32},{32,64},{64,96},{96,0},{1,33},{33,65},{65,97},{97,1},{2,34}... | collective-permute-start | bytes 147464 | tf_op jit(solution)/shard_map/ppermute | solution.py:460
  58.9 3.7 %collective-permute-start.13 = (bf16[96,256]{1,0:T(8,128)(2,1)S(1)}, bf16[96,256]{1,0:T(8,128)(2,1)S(1)}, u32[]{:S(2)}, u32[]{:S(2)}) collective-permute-start(bf16[96,256]{1,0:T(8,128)(2,1)S(1)} %collective-permute-done.12.c_ref), channel_id=1, source_target_pairs={{0,1},{1,0},{2,3},{3,2},{4,5},{5,4},{6,7},{7,6},{8,9},{9,8},{10,11... | collective-permute-start | bytes 147464 | tf_op jit(solution)/shard_map/ppermute | solution.py:361
  61.7 1.2 %collective-permute-start.11 = (bf16[96,256]{1,0:T(8,128)(2,1)S(1)}, bf16[96,256]{1,0:T(8,128)(2,1)S(1)}, u32[]{:S(2)}, u32[]{:S(2)}) collective-permute-start(bf16[96,256]{1,0:T(8,128)(2,1)S(1)} %collective-permute-done.10.a_ref), channel_id=1, source_target_pairs={{0,1},{1,0},{2,3},{3,2},{4,5},{5,4},{6,7},{7,6},{8,9},{9,8},{10,11... | collective-permute-start | bytes 147464 | tf_op jit(solution)/shard_map/ppermute | solution.py:361
  64.4 1.3 %collective-permute-start.14 = (bf16[96,256]{1,0:T(8,128)(2,1)S(1)}, bf16[96,256]{1,0:T(8,128)(2,1)S(1)}, u32[]{:S(2)}, u32[]{:S(2)}) collective-permute-start(bf16[96,256]{1,0:T(8,128)(2,1)S(1)} %get-tuple-element.32), channel_id=1, source_target_pairs={{0,1},{1,0},{2,3},{3,2},{4,5},{5,4},{6,7},{7,6},{8,9},{9,8},{10,11... | collective-permute-start | bytes 147464 | tf_op jit(solution)/shard_map/ppermute | solution.py:361
  65.7 1.3 %collective-permute-start.17 = (bf16[96,256]{1,0:T(8,128)(2,1)S(1)}, bf16[96,256]{1,0:T(8,128)(2,1)S(1)}, u32[]{:S(2)}, u32[]{:S(2)}) collective-permute-start(bf16[96,256]{1,0:T(8,128)(2,1)S(1)} %add_convert_fusion.6), channel_id=1, source_target_pairs={{0,1},{1,0},{2,3},{3,2},{4,5},{5,4},{6,7},{7,6},{32,38},{33,39},{3... | collective-permute-start | bytes 147464 | tf_op jit(solution)/shard_map/ppermute | solution.py:454
  65.9 1.2 %collective-permute-start.16 = (bf16[96,256]{1,0:T(8,128)(2,1)S(1)}, bf16[96,256]{1,0:T(8,128)(2,1)S(1)}, u32[]{:S(2)}, u32[]{:S(2)}) collective-permute-start(bf16[96,256]{1,0:T(8,128)(2,1)S(1)} %add_convert_fusion.6), channel_id=1, source_target_pairs={{0,1},{1,0},{2,3},{3,2},{4,5},{5,4},{6,7},{7,6},{32,36},{33,37},{3... | collective-permute-start | bytes 147464 | tf_op jit(solution)/shard_map/ppermute | solution.py:454
  66.3 1.2 %collective-permute-start.15 = (bf16[96,256]{1,0:T(8,128)(2,1)S(1)}, bf16[96,256]{1,0:T(8,128)(2,1)S(1)}, u32[]{:S(2)}, u32[]{:S(2)}) collective-permute-start(bf16[96,256]{1,0:T(8,128)(2,1)S(1)} %add_convert_fusion.6), channel_id=1, source_target_pairs={{0,1},{1,0},{2,3},{3,2},{4,5},{5,4},{6,7},{7,6},{32,34},{33,35},{3... | collective-permute-start | bytes 147464 | tf_op jit(solution)/shard_map/ppermute | solution.py:454
  67.6 5.1 %collective-permute-start.20 = (bf16[96,256]{1,0:T(8,128)(2,1)S(1)}, bf16[96,256]{1,0:T(8,128)(2,1)S(1)}, u32[]{:S(2)}, u32[]{:S(2)}) collective-permute-start(bf16[96,256]{1,0:T(8,128)(2,1)S(1)} %add_convert_fusion.4), channel_id=1, source_target_pairs={{0,40},{8,32},{32,72},{40,64},{64,104},{72,96},{96,8},{104,0},{1,4... | collective-permute-start | bytes 147464 | tf_op jit(solution)/shard_map/ppermute | solution.py:461
  70.6 4.2 %collective-permute-start.18 = (bf16[96,256]{1,0:T(8,128)(2,1)S(1)}, bf16[96,256]{1,0:T(8,128)(2,1)S(1)}, u32[]{:S(2)}, u32[]{:S(2)}) collective-permute-start(bf16[96,256]{1,0:T(8,128)(2,1)S(1)} %add_convert_fusion.4), channel_id=1, source_target_pairs={{0,32},{32,64},{64,96},{96,0},{1,33},{33,65},{65,97},{97,1},{2,34}... | collective-permute-start | bytes 147464 | tf_op jit(solution)/shard_map/ppermute | solution.py:460
  72.7 5.2 %collective-permute-start.21 = (bf16[96,256]{1,0:T(8,128)(2,1)S(1)}, bf16[96,256]{1,0:T(8,128)(2,1)S(1)}, u32[]{:S(2)}, u32[]{:S(2)}) collective-permute-start(bf16[96,256]{1,0:T(8,128)(2,1)S(1)} %collective-permute-done.20.c_ref), channel_id=1, source_target_pairs={{0,1},{1,0},{2,3},{3,2},{4,5},{5,4},{6,7},{7,6},{8,9},{9,8},{10,11... | collective-permute-start | bytes 147464 | tf_op jit(solution)/shard_map/ppermute | solution.py:361
  74.7 4.1 %collective-permute-start.19 = (bf16[96,256]{1,0:T(8,128)(2,1)S(1)}, bf16[96,256]{1,0:T(8,128)(2,1)S(1)}, u32[]{:S(2)}, u32[]{:S(2)}) collective-permute-start(bf16[96,256]{1,0:T(8,128)(2,1)S(1)} %collective-permute-done.18.a_ref), channel_id=1, source_target_pairs={{0,1},{1,0},{2,3},{3,2},{4,5},{5,4},{6,7},{7,6},{8,9},{9,8},{10,11... | collective-permute-start | bytes 147464 | tf_op jit(solution)/shard_map/ppermute | solution.py:361
  80.2 1.3 %collective-permute-start.22 = (bf16[96,256]{1,0:T(8,128)(2,1)S(1)}, bf16[96,256]{1,0:T(8,128)(2,1)S(1)}, u32[]{:S(2)}, u32[]{:S(2)}) collective-permute-start(bf16[96,256]{1,0:T(8,128)(2,1)S(1)} %get-tuple-element.34), channel_id=1, source_target_pairs={{0,1},{1,0},{2,3},{3,2},{4,5},{5,4},{6,7},{7,6},{8,9},{9,8},{10,11... | collective-permute-start | bytes 147464 | tf_op jit(solution)/shard_map/ppermute | solution.py:361
  81.6 1.3 %collective-permute-start.25 = (bf16[96,256]{1,0:T(8,128)(2,1)S(1)}, bf16[96,256]{1,0:T(8,128)(2,1)S(1)}, u32[]{:S(2)}, u32[]{:S(2)}) collective-permute-start(bf16[96,256]{1,0:T(8,128)(2,1)S(1)} %add_convert_fusion.3), channel_id=1, source_target_pairs={{0,1},{1,0},{2,3},{3,2},{4,5},{5,4},{6,7},{7,6},{32,33},{33,32},{3... | collective-permute-start | bytes 147464 | tf_op jit(solution)/shard_map/ppermute | solution.py:454
  82.0 1.2 %collective-permute-start.24 = (bf16[96,256]{1,0:T(8,128)(2,1)S(1)}, bf16[96,256]{1,0:T(8,128)(2,1)S(1)}, u32[]{:S(2)}, u32[]{:S(2)}) collective-permute-start(bf16[96,256]{1,0:T(8,128)(2,1)S(1)} %add_convert_fusion.3), channel_id=1, source_target_pairs={{0,1},{1,0},{2,3},{3,2},{4,5},{5,4},{6,7},{7,6},{32,33},{33,32},{3... | collective-permute-start | bytes 147464 | tf_op jit(solution)/shard_map/ppermute | solution.py:454
  82.1 1.2 %collective-permute-start.23 = (bf16[96,256]{1,0:T(8,128)(2,1)S(1)}, bf16[96,256]{1,0:T(8,128)(2,1)S(1)}, u32[]{:S(2)}, u32[]{:S(2)}) collective-permute-start(bf16[96,256]{1,0:T(8,128)(2,1)S(1)} %add_convert_fusion.3), channel_id=1, source_target_pairs={{0,1},{1,0},{2,3},{3,2},{4,5},{5,4},{6,7},{7,6},{32,33},{33,32},{3... | collective-permute-start | bytes 147464 | tf_op jit(solution)/shard_map/ppermute | solution.py:454
  83.4 5.3 %collective-permute-start.28 = (bf16[96,256]{1,0:T(8,128)(2,1)S(1)}, bf16[96,256]{1,0:T(8,128)(2,1)S(1)}, u32[]{:S(2)}, u32[]{:S(2)}) collective-permute-start(bf16[96,256]{1,0:T(8,128)(2,1)S(1)} %add_convert_fusion.1), channel_id=1, source_target_pairs={{0,40},{8,32},{32,72},{40,64},{64,104},{72,96},{96,8},{104,0},{1,4... | collective-permute-start | bytes 147464 | tf_op jit(solution)/shard_map/ppermute | solution.py:461
  83.7 6.8 %collective-permute-start.26 = (bf16[96,256]{1,0:T(8,128)(2,1)S(1)}, bf16[96,256]{1,0:T(8,128)(2,1)S(1)}, u32[]{:S(2)}, u32[]{:S(2)}) collective-permute-start(bf16[96,256]{1,0:T(8,128)(2,1)S(1)} %add_convert_fusion.1), channel_id=1, source_target_pairs={{0,32},{32,64},{64,96},{96,0},{1,33},{33,65},{65,97},{97,1},{2,34}... | collective-permute-start | bytes 147464 | tf_op jit(solution)/shard_map/ppermute | solution.py:460
  88.7 2.6 %collective-permute-start.29 = (bf16[96,256]{1,0:T(8,128)(2,1)S(1)}, bf16[96,256]{1,0:T(8,128)(2,1)S(1)}, u32[]{:S(2)}, u32[]{:S(2)}) collective-permute-start(bf16[96,256]{1,0:T(8,128)(2,1)S(1)} %collective-permute-done.28.c_ref), channel_id=1, source_target_pairs={{0,1},{1,0},{2,3},{3,2},{4,5},{5,4},{6,7},{7,6},{8,9},{9,8},{10,11... | collective-permute-start | bytes 147464 | tf_op jit(solution)/shard_map/ppermute | solution.py:361
  90.5 1.2 %collective-permute-start.27 = (bf16[96,256]{1,0:T(8,128)(2,1)S(1)}, bf16[96,256]{1,0:T(8,128)(2,1)S(1)}, u32[]{:S(2)}, u32[]{:S(2)}) collective-permute-start(bf16[96,256]{1,0:T(8,128)(2,1)S(1)} %collective-permute-done.26.a_ref.mine_ref), channel_id=1, source_target_pairs={{0,1},{1,0},{2,3},{3,2},{4,5},{5,4},{6,7},{7,6},{8,9},{9,8},{10,11... | collective-permute-start | bytes 147464 | tf_op jit(solution)/shard_map/ppermute | solution.py:361
  93.1 1.3 %collective-permute-start.30 = (bf16[96,256]{1,0:T(8,128)(2,1)S(1)}, bf16[96,256]{1,0:T(8,128)(2,1)S(1)}, u32[]{:S(2)}, u32[]{:S(2)}) collective-permute-start(bf16[96,256]{1,0:T(8,128)(2,1)S(1)} %get-tuple-element.36), channel_id=1, source_target_pairs={{0,1},{1,0},{2,3},{3,2},{4,5},{5,4},{6,7},{7,6},{8,9},{9,8},{10,11... | collective-permute-start | bytes 147464 | tf_op jit(solution)/shard_map/ppermute | solution.py:361
  94.5 1.3 %collective-permute-start.33 = (bf16[96,256]{1,0:T(8,128)(2,1)S(1)}, bf16[96,256]{1,0:T(8,128)(2,1)S(1)}, u32[]{:S(2)}, u32[]{:S(2)}) collective-permute-start(bf16[96,256]{1,0:T(8,128)(2,1)S(1)} %add_convert_fusion.m0_ref), channel_id=1, source_target_pairs={{0,1},{1,0},{2,3},{3,2},{4,5},{5,4},{6,7},{7,6},{32,33},{33,32},{3... | collective-permute-start | bytes 147464 | tf_op jit(solution)/shard_map/ppermute | solution.py:454
  94.8 1.2 %collective-permute-start.32 = (bf16[96,256]{1,0:T(8,128)(2,1)S(1)}, bf16[96,256]{1,0:T(8,128)(2,1)S(1)}, u32[]{:S(2)}, u32[]{:S(2)}) collective-permute-start(bf16[96,256]{1,0:T(8,128)(2,1)S(1)} %add_convert_fusion.m0_ref), channel_id=1, source_target_pairs={{0,1},{1,0},{2,3},{3,2},{4,5},{5,4},{6,7},{7,6},{32,33},{33,32},{3... | collective-permute-start | bytes 147464 | tf_op jit(solution)/shard_map/ppermute | solution.py:454
  95.0 1.2 %collective-permute-start.31 = (bf16[96,256]{1,0:T(8,128)(2,1)S(1)}, bf16[96,256]{1,0:T(8,128)(2,1)S(1)}, u32[]{:S(2)}, u32[]{:S(2)}) collective-permute-start(bf16[96,256]{1,0:T(8,128)(2,1)S(1)} %add_convert_fusion.m0_ref), channel_id=1, source_target_pairs={{0,1},{1,0},{2,3},{3,2},{4,5},{5,4},{6,7},{7,6},{32,33},{33,32},{3... | collective-permute-start | bytes 147464 | tf_op jit(solution)/shard_map/ppermute | solution.py:454
